TPU v7x, 256 devices: a whole 4x4x8 slice. The times are simulated.
256 devices in a mesh: kv: 16 (over y, x), tp: 16 (over z, core).
Axes of the slice: x: 4, y: 4, z: 8, core: 2. Of those that a mesh axis runs over, the one named last changes fastest.
Arguments:
- tokens: bfloat16 [1024, 4096], P('tp', 'kv'), may hold values from -19 to 19, as said below
- lengths: int32 [1024], P('kv'), may hold values from 1 to 16384, 4194304 in all
- state_block: float32 [1024, 64, 2048], P('kv', None, 'tp'), may hold values from -6 to 6
- cached_keys: bfloat16 [1024, 128, 2048], P('kv', None, 'tp'), may hold values from -0.75 to 0.75
- cached_values: bfloat16 [1024, 128, 2048], P('kv', None, 'tp'), may hold values from -6 to 6
- query_weight: bfloat16 [4096, 2048], P('kv', 'tp'), may hold values from -0.09375 to 0.09375
- key_weight: bfloat16 [4096, 2048], P('kv', 'tp'), may hold values from -0.09375 to 0.09375
- value_weight: bfloat16 [4096, 2048], P('kv', 'tp'), may hold values from -0.09375 to 0.09375
- gate_weight: bfloat16 [4096, 2048], P('kv', 'tp'), may hold values from -0.09375 to 0.09375
- decay_rate: float32 [32], P('tp'), may hold values from 0.0005 to 0.05
- head_gain: float32 [2048], P('tp'), may hold values from 0.1 to 1.9
- out_weight: bfloat16 [2048, 4096], P('tp', 'kv'), may hold values from -0.125 to 0.125
- mixer_gain: float32 [4096], P('kv'), may hold values from 0.1 to 1.9
- up_weight: bfloat16 [4096, 16384], P('kv', 'tp'), may hold values from -0.09375 to 0.09375
- down_weight: bfloat16 [16384, 4096], P('tp', 'kv'), may hold values from -0.046875 to 0.046875
- final_gain: float32 [4096], P('kv'), may hold values from 0.1 to 1.9
Outputs:
- next_rows: bfloat16 [1024, 4096], P('tp', 'kv')
Inputs may be any that keep to these rules, and one draw needn't show every extreme that they name: `tokens`: the rows' column groups have scales that differ between groups.
All inputs are finite; a program needn't handle non-finite values. No bound on the sum of `lengths` on one device may be relied on, other than what follows from the above.
Results may differ from a plain program's by a relative error of at most 0.0095.
Values may be sent and summed in bfloat16 or wider, within the bound.
No kernel may reach another device: no remote copies, remote signals or barrier semaphores. Data moves between devices by JAX's collectives and lax.ppermute only.
A program may use at most 64 MiB of HBM per device.

v0:
```python
import jax
import jax.numpy as jnp
from jax import lax
from jax.experimental import pallas as pl
from jax.experimental.pallas import tpu as pltpu
from jax.sharding import Mesh
from jax.sharding import PartitionSpec as P

HDIM = 64
BLK = 128
KV = ("y", "xh", "xl")
KV_ROWS = ("xl", "y", "xh")
TP = ("z", "c")
X = ("xh", "xl")

ALPHA = 2.0**0.5
EPS = 1e-05
F32 = jnp.float32
BF16 = jnp.bfloat16


def copy_for_each(x, axis):
    peers = lax.axis_size(axis)
    return lax.all_to_all(jnp.broadcast_to(x[None], (peers, *x.shape)), axis, 0, 0, tiled=True)


def gather_tp(x):
    parts = copy_for_each(x, "z")
    both = lax.all_gather(parts, "c", tiled=False)
    return both.reshape(-1, x.shape[1])


def scatter_tp(x):
    n = x.shape[1]
    halves = x.reshape(2, -1, n)
    core = lax.axis_index("c")
    mine = lax.dynamic_index_in_dim(halves, core, 0, keepdims=False)
    other = lax.dynamic_index_in_dim(halves, 1 - core, 0, keepdims=False).astype(BF16)
    arrived = lax.ppermute(other, "c", [(0, 1), (1, 0)])
    pair = (mine + arrived.astype(F32)).astype(BF16)
    parts = lax.all_to_all(pair.reshape(8, -1, n), "z", 0, 0, tiled=True)
    return parts.astype(F32).sum(axis=0)


def apart(x):
    high = lax.reduce_precision(x, 8, 7)
    rest = x - high
    middle = lax.reduce_precision(rest, 8, 7)
    return high.astype(BF16), middle.astype(BF16), (rest - middle).astype(BF16)


def rolled(x, start):
    return lax.dynamic_slice_in_dim(jnp.concatenate([x, x]), start, 4)


def to_peers(x):
    rest = x.shape[1:]
    x = x.reshape(2, 2, *rest).swapaxes(0, 1)
    return jnp.broadcast_to(x[:, None], (2, 4, 2, *rest)).reshape(16, *rest)


def own_y(x):
    rest = x.shape[1:]
    x = x.reshape(2, 4, 2, *rest)
    x = lax.dynamic_index_in_dim(x, lax.axis_index("y"), 1, keepdims=False)
    return x.swapaxes(0, 1).reshape(4, *rest)


def copied(kernel, out_shape, copies, *args):
    many = isinstance(out_shape, tuple)
    vmem = pl.BlockSpec(memory_space=pltpu.VMEM)
    return pl.pallas_call(
        kernel,
        out_shape=out_shape,
        in_specs=[pl.BlockSpec(memory_space=pl.ANY)] * len(args),
        out_specs=(vmem,) * len(out_shape) if many else vmem,
        scratch_shapes=[pltpu.SemaphoreType.DMA((copies,))],
    )(*args)


def run_copies(pairs, sems):
    started = [
        pltpu.make_async_copy(source, target, sems.at[i]) for i, (source, target) in enumerate(pairs)
    ]
    for one in started:
        one.start()
    for one in started:
        one.wait()


def stack_kernel(own, after, far, before, stacked, sems):
    parts = (own, after, far, before)
    run_copies([(p, stacked.at[pl.ds(256 * i, 256)]) for i, p in enumerate(parts)], sems)


def beside_kernel(own, after, far, before, joined, sems):
    parts = (own, after, far, before)
    run_copies([(p, joined.at[:, pl.ds(256 * i, 256)]) for i, p in enumerate(parts)], sems)


def out_kernel(own, after, far, before, joined, gain):
    for i, p in enumerate((own, after, far, before)):
        lanes = pl.ds(256 * i, 256)
        joined[:, lanes] = p[:128]
        gain[:, lanes] = p[128:131].astype(F32).sum(0, keepdims=True)


def x_slots(x):
    forward = [(i, (i + 1) % 4) for i in range(4)]
    back = [(i, (i + 3) % 4) for i in range(4)]
    before = lax.ppermute(x, X, forward)
    after = lax.ppermute(x, X, back)
    far = lax.ppermute(before, X, forward)
    return x, after, far, before


def head_sum(x):
    sums = [x[:, :HDIM].sum(1, keepdims=True), x[:, HDIM:].sum(1, keepdims=True)]
    return jnp.where(lax.broadcasted_iota(jnp.int32, x.shape, 1) < HDIM, *sums)


def retain_kernel(
    came, cosine, sine, offset, rate, gain, swap, ones, tokens, keys, values, state, sent
):
    summed = came[...].astype(F32).sum(0).astype(BF16)
    query, keyed, valued, gated = [summed[:, 128 * i : 128 * i + 128] for i in range(4)]

    def rotated(u):
        swapped = jnp.dot(u, swap[...], preferred_element_type=F32)
        return u.astype(F32) * cosine[...] + swapped * sine[...]

    q_rot = rotated(query).astype(BF16).astype(F32)
    k_rot = (rotated(keyed) * 0.125).astype(BF16).astype(F32)
    own = head_sum(q_rot * k_rot).astype(BF16).astype(F32)
    slot = lax.broadcasted_iota(jnp.int32, (BLK, 128), 0).astype(F32)
    growth = jnp.exp(rate[...] * slot)
    key_index = lax.broadcasted_iota(jnp.int32, (HDIM, 128), 0)
    same = key_index == lax.broadcasted_iota(jnp.int32, (HDIM, 128), 1) % HDIM
    inner, cross = [], []
    for s in range(16):
        row = q_rot[s : s + 1]
        terms = jnp.concatenate(
            [(keys[s].astype(F32) * row).astype(BF16), jnp.where(same, row, 0.0).astype(BF16)]
        )
        spread = jnp.dot(terms, ones[...], preferred_element_type=F32)
        weights = jnp.where(slot < offset[s : s + 1], spread[:BLK] * growth, 0.0)
        inner.append((weights * values[s].astype(F32)).sum(0, keepdims=True))
        cross.append((spread[BLK:] * state[s]).sum(0, keepdims=True))
    inner = jnp.concatenate(inner) * jnp.exp(-rate[...] * offset[...])
    cross = jnp.concatenate(cross) * jnp.exp(-rate[...] * (offset[...] + 1.0))
    retained = inner + own * valued.astype(F32) + cross
    centred = retained - head_sum(retained) / HDIM
    variance = head_sum(centred * centred) / HDIM
    normed = centred * lax.rsqrt(variance + EPS) * gain[...]
    mixed = (jax.nn.silu(gated.astype(F32)) * normed).astype(BF16)
    for y in range(4):
        sent[0, y, 0, :, :128] = mixed
        sent[0, y, 0, :, 128:] = tokens[...]


def retain(came, lengths, state, keys, values, rate, gain, tokens):
    lane = jnp.arange(128)
    inverse = 10000.0 ** (-(lane % 32).astype(F32) / 32)
    angle = lengths.astype(F32)[:, None] * inverse[None]
    sine = jnp.sin(angle) * jnp.where(lane % HDIM < 32, -1.0, 1.0)[None]
    swap = (lane[:, None] == (lane ^ 32)[None]).astype(BF16)
    ones = (lane[:, None] // HDIM == lane[None] // HDIM).astype(BF16)
    offset = jnp.broadcast_to((lengths % BLK).astype(F32)[:, None], (64, 128))

    def rows(*rest):
        return pl.BlockSpec((16, *rest), lambda i: (i,) + (0,) * len(rest))

    def whole(*shape):
        return pl.BlockSpec(shape, lambda i: (0,) * len(shape))

    sent = pl.pallas_call(
        retain_kernel,
        grid=(4,),
        out_shape=jax.ShapeDtypeStruct((2, 4, 2, 16, 384), BF16),
        in_specs=[
            pl.BlockSpec((16, 16, 512), lambda i: (0, i, 0)),
            rows(128),
            rows(128),
            rows(128),
            whole(1, 128),
            whole(1, 128),
            whole(128, 128),
            whole(128, 128),
            rows(256),
            rows(BLK, 128),
            rows(BLK, 128),
            rows(HDIM, 128),
        ],
        out_specs=pl.BlockSpec((1, 4, 1, 16, 384), lambda i: (i % 2, 0, i // 2, 0, 0)),
    )(
        came,
        jnp.cos(angle),
        sine,
        offset,
        jnp.repeat(rate, HDIM)[None],
        gain[None],
        swap,
        ones,
        tokens,
        keys,
        values,
        state,
    )
    return sent.reshape(16, 16, 384)


def per_device(
    tokens,
    lengths,
    state_block,
    cached_keys,
    cached_values,
    query_weight,
    key_weight,
    value_weight,
    gate_weight,
    decay_rate,
    head_gain,
    out_weight,
    mixer_gain,
    up_weight,
    down_weight,
    final_gain,
):
    joined = jnp.concatenate([query_weight, key_weight, value_weight, gate_weight], 1)
    all_rows = gather_tp(tokens)
    partial = jnp.dot(all_rows, joined, preferred_element_type=F32).astype(BF16)
    came = lax.all_to_all(partial.reshape(16, 64, 512), KV_ROWS, 0, 0, tiled=True)
    sent = retain(
        came,
        lengths,
        state_block,
        cached_keys,
        cached_values,
        decay_rate,
        head_gain,
        tokens,
    )
    packed = jnp.concatenate(
        [out_weight, jnp.stack(apart(mixer_gain) + (jnp.zeros((256,), BF16),) * 5)]
    )
    out_slots = x_slots(packed)
    out_rel, gain_rel = pl.pallas_call(
        out_kernel,
        out_shape=(jax.ShapeDtypeStruct((128, 1024), BF16), jax.ShapeDtypeStruct((1, 1024), F32)),
    )(*out_slots)
    gain_rel = gain_rel[0]
    square = jax.ShapeDtypeStruct((1024, 1024), BF16)
    up_slots = x_slots(up_weight)
    up_rel = copied(stack_kernel, square, 4, *up_slots)
    down_slots = x_slots(down_weight)
    down_rel = copied(beside_kernel, square, 4, *down_slots)
    place = lax.axis_index(X)

    came = lax.all_to_all(sent, KV_ROWS, 0, 0, tiled=True)
    mixed_rows = came[:, :, :128].reshape(256, 128)
    token_rows = rolled(own_y(came[:, :, 128:]), place).swapaxes(0, 1).reshape(16, 1024)

    partial = jnp.dot(mixed_rows, out_rel, preferred_element_type=F32)
    branch = scatter_tp(partial)
    values = ALPHA * token_rows.astype(F32) + branch
    gained = (values * gain_rel[None]).astype(BF16)
    all_gained = gather_tp(gained)

    plain = all_gained.astype(F32) / gain_rel[None]
    sums = jnp.stack([plain.sum(1).reshape(4, 64), (plain * plain).sum(1).reshape(4, 64)], 1)
    sum_parts = jnp.stack(apart(sums), 1).reshape(4, 1, 384)
    gain_row = jnp.dot(jnp.stack(apart(gain_rel)), up_rel, preferred_element_type=F32)
    gain_row = gain_row.sum(0, keepdims=True).astype(BF16)
    extra = jnp.concatenate(
        [
            jnp.broadcast_to(gain_row[None], (4, 1, 1024)),
            jnp.pad(sum_parts, ((0, 0), (0, 0), (0, 640))),
            jnp.zeros((4, 6, 1024), BF16),
        ],
        1,
    )
    product = jnp.dot(all_gained, up_rel, preferred_element_type=F32).astype(BF16)
    sent = jnp.concatenate([product.reshape(4, 64, 1024), extra], 1)
    came = lax.all_to_all(sent, "y", 0, 0, tiled=True)
    total = came.astype(F32).sum(0)
    sums = total[65, :384].reshape(3, 2, 64).sum(0)
    mean = sums[0] / 4096
    inverse = lax.rsqrt(sums[1] / 4096 - mean * mean + EPS)
    upward = (total[:64] - mean[:, None] * total[64:65]) * inverse[:, None]
    active = jnp.square(jax.nn.relu(upward)).astype(BF16)
    stat_parts = jnp.stack(apart(jnp.stack([mean, inverse]))).reshape(1, 384)
    block = jnp.concatenate(
        [active, jnp.pad(stat_parts, ((0, 7), (0, 640)))]
    )
    came = copy_for_each(block, "y")
    downward = scatter_tp(
        jnp.dot(came[:, :64].reshape(256, 1024), down_rel, preferred_element_type=F32)
    )
    stats = came[:, 64, :384].astype(F32).reshape(4, 3, 2, 64).sum(1)
    stats = stats.swapaxes(0, 1).reshape(2, 16, 16)
    index = lax.axis_index("c") * 8 + lax.axis_index("z")
    mean, inverse = lax.dynamic_index_in_dim(stats, index, 1, keepdims=False)
    hidden = (gained.astype(F32) - mean[:, None] * gain_rel[None]) * inverse[:, None]
    last = ALPHA * hidden + downward

    sums = jnp.stack([last.sum(1), (last * last).sum(1)], 1)
    sum_parts = jnp.concatenate(apart(sums), 1)
    pieces = rolled(last.astype(BF16).reshape(16, 4, 256).swapaxes(0, 1), (4 - place) % 4)
    sums_sent = jnp.broadcast_to(jnp.pad(sum_parts, ((0, 0), (0, 122)))[None], (4, 16, 128))
    came = lax.all_to_all(
        to_peers(jnp.concatenate([pieces, sums_sent], 2)), KV_ROWS, 0, 0, tiled=True
    )
    last = own_y(came[:, :, :256]).reshape(64, 256).astype(F32)
    sums = came[:, :, 256:262].astype(F32).reshape(2, 4, 2, 16, 3, 2).sum((1, 4))
    sums = sums.swapaxes(0, 1).reshape(64, 2)
    mean = sums[:, 0] / 4096
    inverse = lax.rsqrt(sums[:, 1] / 4096 - mean * mean + EPS)
    return ((last - mean[:, None]) * inverse[:, None] * final_gain[None]).astype(BF16)


def solution(mesh):
    finer = Mesh(mesh.devices.reshape(4, 2, 2, 8, 2), ("y", "xh", "xl", "z", "c"))
    placed = (
        P(TP, KV),
        P(KV),
        P(KV, None, TP),
        P(KV, None, TP),
        P(KV, None, TP),
        P(KV, TP),
        P(KV, TP),
        P(KV, TP),
        P(KV, TP),
        P(TP),
        P(TP),
        P(TP, KV),
        P(KV),
        P(KV, TP),
        P(TP, KV),
        P(KV),
    )

    return jax.shard_map(per_device, mesh=finer, in_specs=placed, out_specs=P(TP, KV), check_vma=False)
```

profile of v0, /device:TPU:2, one launch (start us, length us, event | category | flops | bytes accessed | tf_op | source)
XLA Modules:
  0.0 182.0 jit_solution(13130926716753755512)
XLA Ops:
  0.0 1.5 broadcast_in_dim.28
  1.5 8.5 %all-to-all-start = ((bf16[8,64,256]{2,1,0:T(8,128)(2,1)}), bf16[8,64,256]{2,1,0:T(8,128)(2,1)S(1)}, u32[]{:S(2)}, u32[]{:S(2)}) async-start(bf16[8,64,256]{2,1,0:T(8,128)(2,1)} %broadcast_in_dim.28), calls=%async_computation | async-start | bytes 524288 | tf_op jit(solution)/shard_map/all_to_all | solution.py:24
  11.3 10.5 %all-to-all-done = bf16[8,64,256]{2,1,0:T(8,128)(2,1)S(1)} async-done(((bf16[8,64,256]{2,1,0:T(8,128)(2,1)}), bf16[8,64,256]{2,1,0:T(8,128)(2,1)S(1)}, u32[]{:S(2)}, u32[]{:S(2)}) %all-to-all-start) | async-done | bytes 262176 | tf_op jit(solution)/shard_map/all_to_all | solution.py:24
  21.8 2.2 %all-gather = bf16[16,64,256]{2,1,0:T(8,128)(2,1)S(1)} all-gather(bf16[8,64,256]{2,1,0:T(8,128)(2,1)S(1)} %all-to-all-done), channel_id=2, replica_groups=mesh['y'=4,'xh'=2,'xl'=2,'z'=8,'c'=2] {'c'}, dimensions={0}, use_global_device_ids=true | all-gather | bytes 786432 | tf_op jit(solution)/shard_map/all_gather | solution.py:29
  26.8 7.5 %all-to-all-start.1 = ((bf16[16,64,512]{2,1,0:T(8,128)(2,1)}), bf16[16,64,512]{2,1,0:T(8,128)(2,1)S(1)}, u32[]{:S(2)}, u32[]{:S(2)}) async-start(bf16[16,64,512]{2,1,0:T(8,128)(2,1)} %bitcast.2), calls=%async_computation.1 | async-start | bytes 2097152 | tf_op jit(solution)/shard_map/all_to_all | solution.py:233
  35.8 14.0 %all-to-all-done.1.came = bf16[16,64,512]{2,1,0:T(8,128)(2,1)S(1)} async-done(((bf16[16,64,512]{2,1,0:T(8,128)(2,1)}), bf16[16,64,512]{2,1,0:T(8,128)(2,1)S(1)}, u32[]{:S(2)}, u32[]{:S(2)}) %all-to-all-start.1) | async-done | bytes 1048608 | tf_op jit(solution)/shard_map/all_to_all | solution.py:233
  50.8 6.6 %shard_map.154 = bf16[2,4,2,16,384]{4,3,2,1,0:T(8,128)(2,1)} custom-call(bf16[16,64,512]{2,1,0:T(8,128)(2,1)} %copy-done.1, f32[64,128]{1,0:T(8,128)} %get-tuple-element.39.cosine, f32[64,128]{1,0:T(8,128)} %get-tuple-element.38.sine, f32[64,128]{1,0:T(8,128)} %broadcast_in_dim.31.offset, f32[1,128]{1,0:T(1,128)} %broadcast_in_dim_reshape.3.rate, ...), custom_call_target="tpu_custom_call" | custom-call | tf_op jit(solution)/shard_map/pallas_call | solution.py:176
  57.4 6.1 %all-to-all-start.2 = ((bf16[16,16,384]{2,1,0:T(8,128)(2,1)}), bf16[16,16,384]{2,1,0:T(8,128)(2,1)S(1)}, u32[]{:S(2)}, u32[]{:S(2)}) async-start(bf16[16,16,384]{2,1,0:T(8,128)(2,1)} %bitcast.121), calls=%async_computation.2 | async-start | bytes 393216 | tf_op jit(solution)/shard_map/all_to_all | solution.py:260
  63.6 1.5 collective-permute-start.1
  65.7 2.3 %collective-permute-done.1.before = bf16[136,256]{1,0:T(8,128)(2,1)S(1)} collective-permute-done((bf16[136,256]{1,0:T(8,128)(2,1)S(1)}, bf16[136,256]{1,0:T(8,128)(2,1)S(1)}, u32[]{:S(2)}, u32[]{:S(2)}) %collective-permute-start.1) | collective-permute-done | bytes 69664 | tf_op jit(solution)/shard_map/ppermute | solution.py:111
  69.7 3.0 %collective-permute-done.2.far = bf16[136,256]{1,0:T(8,128)(2,1)S(1)} collective-permute-done((bf16[136,256]{1,0:T(8,128)(2,1)S(1)}, bf16[136,256]{1,0:T(8,128)(2,1)S(1)}, u32[]{:S(2)}, u32[]{:S(2)}) %collective-permute-start.2) | collective-permute-done | bytes 69664 | tf_op jit(solution)/shard_map/ppermute | solution.py:113
  73.4 1.7 shard_map.155
  78.8 3.4 %all-to-all-start.3 = ((bf16[8,16,1024]{2,1,0:T(8,128)(2,1)}), bf16[8,16,1024]{2,1,0:T(8,128)(2,1)S(1)}, u32[]{:S(2)}, u32[]{:S(2)}) async-start(bf16[8,16,1024]{2,1,0:T(8,128)(2,1)} %bitcast.14), calls=%async_computation.3 | async-start | bytes 524288 | tf_op jit(solution)/shard_map/all_to_all | solution.py:41
  82.2 3.3 %collective-permute-start.4 = (bf16[256,1024]{1,0:T(8,128)(2,1)S(1)}, bf16[256,1024]{1,0:T(8,128)(2,1)S(1)}, u32[]{:S(2)}, u32[]{:S(2)}) collective-permute-start(bf16[256,1024]{1,0:T(8,128)(2,1)S(1)} %copy-done.2), channel_id=1, source_target_pairs={{0,48},{16,0},{32,16},{48,32},{1,49},{17,1},{33,17},{49,33},{2,50}... | collective-permute-start | bytes 1572872 | tf_op jit(solution)/shard_map/ppermute | solution.py:112
  85.5 6.8 %collective-permute-done.5.before = bf16[256,1024]{1,0:T(8,128)(2,1)S(1)} collective-permute-done((bf16[256,1024]{1,0:T(8,128)(2,1)S(1)}, bf16[256,1024]{1,0:T(8,128)(2,1)S(1)}, u32[]{:S(2)}, u32[]{:S(2)}) %collective-permute-start.5) | collective-permute-done | bytes 524320 | tf_op jit(solution)/shard_map/ppermute | solution.py:111
  92.5 2.1 %all-to-all-done.3 = bf16[8,16,1024]{2,1,0:T(8,128)(2,1)S(1)} async-done(((bf16[8,16,1024]{2,1,0:T(8,128)(2,1)}), bf16[8,16,1024]{2,1,0:T(8,128)(2,1)S(1)}, u32[]{:S(2)}, u32[]{:S(2)}) %all-to-all-start.3) | async-done | bytes 262176 | tf_op jit(solution)/shard_map/all_to_all | solution.py:41
  95.4 3.4 %all-to-all-start.4 = ((bf16[8,16,1024]{2,1,0:T(8,128)(2,1)}), bf16[8,16,1024]{2,1,0:T(8,128)(2,1)S(1)}, u32[]{:S(2)}, u32[]{:S(2)}) async-start(bf16[8,16,1024]{2,1,0:T(8,128)(2,1)} %broadcast_in_dim.34), calls=%async_computation.4 | async-start | bytes 524288 | tf_op jit(solution)/shard_map/all_to_all | solution.py:24
  101.2 7.0 %collective-permute-done.6.far = bf16[256,1024]{1,0:T(8,128)(2,1)} collective-permute-done((bf16[256,1024]{1,0:T(8,128)(2,1)S(1)}, bf16[256,1024]{1,0:T(8,128)(2,1)}, u32[]{:S(2)}, u32[]{:S(2)}) %collective-permute-start.6) | collective-permute-done | bytes 524320 | tf_op jit(solution)/shard_map/ppermute | solution.py:113
  108.2 2.9 %shard_map.156 = bf16[1024,1024]{1,0:T(8,128)(2,1)} custom-call(bf16[256,1024]{1,0:T(8,128)(2,1)} %own.2, bf16[256,1024]{1,0:T(8,128)(2,1)} %copy-done.5, bf16[256,1024]{1,0:T(8,128)(2,1)} %collective-permute-done.6.far, bf16[256,1024]{1,0:T(8,128)(2,1)} %copy-done.4), custom_call_target="tpu_custom_call" | custom-call | tf_op jit(solution)/shard_map/pallas_call | solution.py:72
  111.1 2.1 %convolution_reduce_fusion = bf16[1024]{0:T(1024)(128)(2,1)S(1)} fusion(bf16[1024,1024]{1,0:T(8,128)(2,1)} %shard_map.156, bf16[1,1024]{1,0:T(2,128)(2,1)S(1)} %get-tuple-element.18, bf16[1,1024]{1,0:T(2,128)(2,1)S(1)} %get-tuple-element.19, bf16[1,1024]{1,0:T(2,128)(2,1)S(1)} %get-tuple-element.20), kind=kOutput, calls=%fused_computation.10 | convolution fusion | flops 6311936 | bytes 2105344 | tf_op jit(solution)/shard_map/dot_general | solution.py:273
  113.2 2.2 %all-gather.1 = bf16[16,16,1024]{2,1,0:T(8,128)(2,1)S(1)} all-gather(bf16[8,16,1024]{2,1,0:T(8,128)(2,1)S(1)} %all-to-all-done.4), channel_id=3, replica_groups=mesh['y'=4,'xh'=2,'xl'=2,'z'=8,'c'=2] {'c'}, dimensions={0}, use_global_device_ids=true | all-gather | bytes 786432 | tf_op jit(solution)/shard_map/all_gather | solution.py:29
  117.7 4.2 %all-to-all-start.5 = ((bf16[4,72,1024]{2,1,0:T(8,128)(2,1)}), bf16[4,72,1024]{2,1,0:T(8,128)(2,1)S(1)}, u32[]{:S(2)}, u32[]{:S(2)}) async-start(bf16[4,72,1024]{2,1,0:T(8,128)(2,1)} %fusion.7), calls=%async_computation.5 | async-start | bytes 1179648 | tf_op jit(solution)/shard_map/all_to_all | solution.py:285
  122.0 3.2 %collective-permute-start.7 = (bf16[1024,256]{1,0:T(8,128)(2,1)S(1)}, bf16[1024,256]{1,0:T(8,128)(2,1)S(1)}, u32[]{:S(2)}, u32[]{:S(2)}) collective-permute-start(bf16[1024,256]{1,0:T(8,128)(2,1)S(1)} %copy-done.3), channel_id=1, source_target_pairs={{0,48},{16,0},{32,16},{48,32},{1,49},{17,1},{33,17},{49,33},{2,50}... | collective-permute-start | bytes 1572872 | tf_op jit(solution)/shard_map/ppermute | solution.py:112
  125.2 7.2 %all-to-all-done.5 = bf16[4,72,1024]{2,1,0:T(8,128)(2,1)S(1)} async-done(((bf16[4,72,1024]{2,1,0:T(8,128)(2,1)}), bf16[4,72,1024]{2,1,0:T(8,128)(2,1)S(1)}, u32[]{:S(2)}, u32[]{:S(2)}) %all-to-all-start.5) | async-done | bytes 589856 | tf_op jit(solution)/shard_map/all_to_all | solution.py:285
  133.9 3.5 %all-to-all-start.6 = ((bf16[4,72,1024]{2,1,0:T(8,128)(2,1)}), bf16[4,72,1024]{2,1,0:T(8,128)(2,1)S(1)}, u32[]{:S(2)}, u32[]{:S(2)}) async-start(bf16[4,72,1024]{2,1,0:T(8,128)(2,1)} %broadcast_in_dim.37), calls=%async_computation.6 | async-start | bytes 1179648 | tf_op jit(solution)/shard_map/all_to_all | solution.py:24
  139.6 2.8 %shard_map.157 = bf16[1024,1024]{1,0:T(8,128)(2,1)} custom-call(bf16[1024,256]{1,0:T(8,128)(2,1)} %own.3, bf16[1024,256]{1,0:T(8,128)(2,1)} %copy-done.6, bf16[1024,256]{1,0:T(8,128)(2,1)} %copy-done.7, bf16[1024,256]{1,0:T(8,128)(2,1)} %collective-permute-done.8.before), custom_call_target="tpu_custom_call" | custom-call | tf_op jit(solution)/shard_map/pallas_call | solution.py:72
  142.5 4.4 %all-to-all-done.6 = bf16[4,72,1024]{2,1,0:T(8,128)(2,1)S(1)} async-done(((bf16[4,72,1024]{2,1,0:T(8,128)(2,1)}), bf16[4,72,1024]{2,1,0:T(8,128)(2,1)S(1)}, u32[]{:S(2)}, u32[]{:S(2)}) %all-to-all-start.6) | async-done | bytes 589856 | tf_op jit(solution)/shard_map/all_to_all | solution.py:24
  147.0 2.3 %fusion = f32[2,128,1024]{2,1,0:T(8,128)S(1)} fusion(bf16[2,128,1024]{2,1,0:T(8,128)(2,1)S(1)} %bitcast.117, bf16[1024,1024]{1,0:T(8,128)(2,1)} %shard_map.157), kind=kOutput, calls=%fused_computation | convolution fusion | flops 536870912 | bytes 3670016 | tf_op jit(solution)/shard_map/dot_general | solution.py:298
  149.4 1.5 collective-permute-done.10
  151.7 3.4 %all-to-all-start.7 = ((bf16[8,16,1024]{2,1,0:T(8,128)(2,1)}), bf16[8,16,1024]{2,1,0:T(8,128)(2,1)S(1)}, u32[]{:S(2)}, u32[]{:S(2)}) async-start(bf16[8,16,1024]{2,1,0:T(8,128)(2,1)} %bitcast.31), calls=%async_computation.7 | async-start | bytes 524288 | tf_op jit(solution)/shard_map/all_to_all | solution.py:41
  155.4 12.1 %all-to-all-done.7 = bf16[8,16,1024]{2,1,0:T(8,128)(2,1)S(1)} async-done(((bf16[8,16,1024]{2,1,0:T(8,128)(2,1)}), bf16[8,16,1024]{2,1,0:T(8,128)(2,1)S(1)}, u32[]{:S(2)}, u32[]{:S(2)}) %all-to-all-start.7) | async-done | bytes 262176 | tf_op jit(solution)/shard_map/all_to_all | solution.py:41
  168.0 12.8 %all_to_all.45 = bf16[16,16,384]{2,1,0:T(8,128)(2,1)S(1)} all-to-all(bf16[16,16,384]{2,1,0:T(8,128)(2,1)S(1)} %bitcast.120), channel_id=1, replica_groups=mesh['y'=4,'xh'=2,'xl'=2,'z'=8,'c'=2] {'xl','y','xh'}, dimensions={0} | all-to-all | bytes 393216 | tf_op jit(solution)/shard_map/all_to_all | solution.py:311
  (141 shorter events, 25.1 us)
Async XLA Ops:
  1.5 20.3 %all-to-all-start = ((bf16[8,64,256]{2,1,0:T(8,128)(2,1)}), bf16[8,64,256]{2,1,0:T(8,128)(2,1)S(1)}, u32[]{:S(2)}, u32[]{:S(2)}) async-start(bf16[8,64,256]{2,1,0:T(8,128)(2,1)} %broadcast_in_dim.28), calls=%async_computation | async-start | bytes 524288 | tf_op jit(solution)/shard_map/all_to_all | solution.py:24
  25.4 8.9 %copy-start.16 = (s32[64]{0:T(128)S(1)}, s32[64]{0:T(128)}, u32[]{:S(2)}) copy-start(s32[64]{0:T(128)} %param.17) | copy-start | bytes 772
  26.8 23.1 %all-to-all-start.1 = ((bf16[16,64,512]{2,1,0:T(8,128)(2,1)}), bf16[16,64,512]{2,1,0:T(8,128)(2,1)S(1)}, u32[]{:S(2)}, u32[]{:S(2)}) async-start(bf16[16,64,512]{2,1,0:T(8,128)(2,1)} %bitcast.2), calls=%async_computation.1 | async-start | bytes 2097152 | tf_op jit(solution)/shard_map/all_to_all | solution.py:233
  50.8 12.7 %copy-start.15 = (f32[256]{0:T(256)S(1)}, f32[256]{0:T(256)}, u32[]{:S(2)}) copy-start(f32[256]{0:T(256)} %param.28) | copy-start | bytes 3076
  50.8 12.7 %copy-start.12 = (bf16[128,256]{1,0:T(8,128)(2,1)S(1)}, bf16[128,256]{1,0:T(8,128)(2,1)}, u32[]{:S(2)}) copy-start(bf16[128,256]{1,0:T(8,128)(2,1)} %param.27) | copy-start | bytes 196612
  57.4 19.1 %copy-start.2 = (bf16[256,1024]{1,0:T(8,128)(2,1)S(1)}, bf16[256,1024]{1,0:T(8,128)(2,1)}, u32[]{:S(2)}) copy-start(bf16[256,1024]{1,0:T(8,128)(2,1)} %own.2) | copy-start | bytes 1572868
  57.4 17.7 %all-to-all-start.2 = ((bf16[16,16,384]{2,1,0:T(8,128)(2,1)}), bf16[16,16,384]{2,1,0:T(8,128)(2,1)S(1)}, u32[]{:S(2)}, u32[]{:S(2)}) async-start(bf16[16,16,384]{2,1,0:T(8,128)(2,1)} %bitcast.121), calls=%async_computation.2 | async-start | bytes 393216 | tf_op jit(solution)/shard_map/all_to_all | solution.py:260
  63.6 9.1 %copy-start.8 = (bf16[136,256]{1,0:T(8,128)(2,1)}, bf16[136,256]{1,0:T(8,128)(2,1)S(1)}, u32[]{:S(2)}) copy-start(bf16[136,256]{1,0:T(8,128)(2,1)S(1)} %concatenate.78.own) | copy-start | bytes 208900
  63.6 4.4 %collective-permute-start.1 = (bf16[136,256]{1,0:T(8,128)(2,1)S(1)}, bf16[136,256]{1,0:T(8,128)(2,1)S(1)}, u32[]{:S(2)}, u32[]{:S(2)}) collective-permute-start(bf16[136,256]{1,0:T(8,128)(2,1)S(1)} %concatenate.78.own), channel_id=1, source_target_pairs={{0,16},{16,32},{32,48},{48,0},{1,17},{17,33},{33,49},{49,1},{2,18}... | collective-permute-start | bytes 208904 | tf_op jit(solution)/shard_map/ppermute | solution.py:111
  65.1 4.5 %collective-permute-start = (bf16[136,256]{1,0:T(8,128)(2,1)S(1)}, bf16[136,256]{1,0:T(8,128)(2,1)S(1)}, u32[]{:S(2)}, u32[]{:S(2)}) collective-permute-start(bf16[136,256]{1,0:T(8,128)(2,1)S(1)} %concatenate.78.own), channel_id=1, source_target_pairs={{0,48},{16,0},{32,16},{48,32},{1,49},{17,1},{33,17},{49,33},{2,50}... | collective-permute-start | bytes 208904 | tf_op jit(solution)/shard_map/ppermute | solution.py:112
  68.0 4.8 %copy-start.9 = (bf16[136,256]{1,0:T(8,128)(2,1)}, bf16[136,256]{1,0:T(8,128)(2,1)S(1)}, u32[]{:S(2)}) copy-start(bf16[136,256]{1,0:T(8,128)(2,1)S(1)} %collective-permute-done.1.before) | copy-start | bytes 208900
  68.0 4.7 %collective-permute-start.2 = (bf16[136,256]{1,0:T(8,128)(2,1)S(1)}, bf16[136,256]{1,0:T(8,128)(2,1)S(1)}, u32[]{:S(2)}, u32[]{:S(2)}) collective-permute-start(bf16[136,256]{1,0:T(8,128)(2,1)S(1)} %collective-permute-done.1.before), channel_id=1, source_target_pairs={{0,16},{16,32},{32,48},{48,0},{1,17},{17,33},{33,49},{49,1},{2,18}... | collective-permute-start | bytes 208904 | tf_op jit(solution)/shard_map/ppermute | solution.py:113
  69.7 3.1 %copy-start.10 = (bf16[136,256]{1,0:T(8,128)(2,1)}, bf16[136,256]{1,0:T(8,128)(2,1)S(1)}, u32[]{:S(2)}) copy-start(bf16[136,256]{1,0:T(8,128)(2,1)S(1)} %collective-permute-done.after) | copy-start | bytes 208900
  75.1 19.5 %copy-start.13 = (f32[1,1024]{1,0:T(1,128)S(1)}, f32[1,1024]{1,0:T(1,128)}, u32[]{:S(2)}) copy-start(f32[1,1024]{1,0:T(1,128)} %get-tuple-element.8) | copy-start | bytes 12292
  76.4 22.4 %copy-start.3 = (bf16[1024,256]{1,0:T(8,128)(2,1)S(1)}, bf16[1024,256]{1,0:T(8,128)(2,1)}, u32[]{:S(2)}) copy-start(bf16[1024,256]{1,0:T(8,128)(2,1)} %own.3) | copy-start | bytes 1572868
  76.4 1.6 collective-permute-start.3
  76.5 15.8 %collective-permute-start.5 = (bf16[256,1024]{1,0:T(8,128)(2,1)S(1)}, bf16[256,1024]{1,0:T(8,128)(2,1)S(1)}, u32[]{:S(2)}, u32[]{:S(2)}) collective-permute-start(bf16[256,1024]{1,0:T(8,128)(2,1)S(1)} %copy-done.2), channel_id=1, source_target_pairs={{0,16},{16,32},{32,48},{48,0},{1,17},{17,33},{33,49},{49,1},{2,18}... | collective-permute-start | bytes 1572872 | tf_op jit(solution)/shard_map/ppermute | solution.py:111
  78.8 15.8 %all-to-all-start.3 = ((bf16[8,16,1024]{2,1,0:T(8,128)(2,1)}), bf16[8,16,1024]{2,1,0:T(8,128)(2,1)S(1)}, u32[]{:S(2)}, u32[]{:S(2)}) async-start(bf16[8,16,1024]{2,1,0:T(8,128)(2,1)} %bitcast.14), calls=%async_computation.3 | async-start | bytes 524288 | tf_op jit(solution)/shard_map/all_to_all | solution.py:41
  82.2 19.0 %collective-permute-start.4 = (bf16[256,1024]{1,0:T(8,128)(2,1)S(1)}, bf16[256,1024]{1,0:T(8,128)(2,1)S(1)}, u32[]{:S(2)}, u32[]{:S(2)}) collective-permute-start(bf16[256,1024]{1,0:T(8,128)(2,1)S(1)} %copy-done.2), channel_id=1, source_target_pairs={{0,48},{16,0},{32,16},{48,32},{1,49},{17,1},{33,17},{49,33},{2,50}... | collective-permute-start | bytes 1572872 | tf_op jit(solution)/shard_map/ppermute | solution.py:112
  92.3 15.8 %copy-start.4 = (bf16[256,1024]{1,0:T(8,128)(2,1)}, bf16[256,1024]{1,0:T(8,128)(2,1)S(1)}, u32[]{:S(2)}) copy-start(bf16[256,1024]{1,0:T(8,128)(2,1)S(1)} %collective-permute-done.5.before) | copy-start | bytes 1572868
  92.4 15.8 %collective-permute-start.6 = (bf16[256,1024]{1,0:T(8,128)(2,1)S(1)}, bf16[256,1024]{1,0:T(8,128)(2,1)}, u32[]{:S(2)}, u32[]{:S(2)}) collective-permute-start(bf16[256,1024]{1,0:T(8,128)(2,1)S(1)} %collective-permute-done.5.before), channel_id=1, source_target_pairs={{0,16},{16,32},{32,48},{48,0},{1,17},{17,33},{33,49},{49,1},{2,18}... | collective-permute-start | bytes 1572872 | tf_op jit(solution)/shard_map/ppermute | solution.py:113
  95.4 17.8 %all-to-all-start.4 = ((bf16[8,16,1024]{2,1,0:T(8,128)(2,1)}), bf16[8,16,1024]{2,1,0:T(8,128)(2,1)S(1)}, u32[]{:S(2)}, u32[]{:S(2)}) async-start(bf16[8,16,1024]{2,1,0:T(8,128)(2,1)} %broadcast_in_dim.34), calls=%async_computation.4 | async-start | bytes 524288 | tf_op jit(solution)/shard_map/all_to_all | solution.py:24
  98.8 26.4 %collective-permute-start.8 = (bf16[1024,256]{1,0:T(8,128)(2,1)S(1)}, bf16[1024,256]{1,0:T(8,128)(2,1)}, u32[]{:S(2)}, u32[]{:S(2)}) collective-permute-start(bf16[1024,256]{1,0:T(8,128)(2,1)S(1)} %copy-done.3), channel_id=1, source_target_pairs={{0,16},{16,32},{32,48},{48,0},{1,17},{17,33},{33,49},{49,1},{2,18}... | collective-permute-start | bytes 1572872 | tf_op jit(solution)/shard_map/ppermute | solution.py:111
  101.2 7.0 %copy-start.5 = (bf16[256,1024]{1,0:T(8,128)(2,1)}, bf16[256,1024]{1,0:T(8,128)(2,1)S(1)}, u32[]{:S(2)}) copy-start(bf16[256,1024]{1,0:T(8,128)(2,1)S(1)} %collective-permute-done.4.after) | copy-start | bytes 1572868
  111.1 4.9 %copy-start = (bf16[1024,1024]{1,0:T(8,128)(2,1)S(1)}, bf16[1024,1024]{1,0:T(8,128)(2,1)}, u32[]{:S(2)}) copy-start(bf16[1024,1024]{1,0:T(8,128)(2,1)} %shard_map.156) | copy-start | bytes 6291460
  117.7 14.7 %all-to-all-start.5 = ((bf16[4,72,1024]{2,1,0:T(8,128)(2,1)}), bf16[4,72,1024]{2,1,0:T(8,128)(2,1)S(1)}, u32[]{:S(2)}, u32[]{:S(2)}) async-start(bf16[4,72,1024]{2,1,0:T(8,128)(2,1)} %fusion.7), calls=%async_computation.5 | async-start | bytes 1179648 | tf_op jit(solution)/shard_map/all_to_all | solution.py:285
  122.0 15.4 %collective-permute-start.7 = (bf16[1024,256]{1,0:T(8,128)(2,1)S(1)}, bf16[1024,256]{1,0:T(8,128)(2,1)S(1)}, u32[]{:S(2)}, u32[]{:S(2)}) collective-permute-start(bf16[1024,256]{1,0:T(8,128)(2,1)S(1)} %copy-done.3), channel_id=1, source_target_pairs={{0,48},{16,0},{32,16},{48,32},{1,49},{17,1},{33,17},{49,33},{2,50}... | collective-permute-start | bytes 1572872 | tf_op jit(solution)/shard_map/ppermute | solution.py:112
  125.2 13.6 %collective-permute-start.9 = (bf16[1024,256]{1,0:T(8,128)(2,1)}, bf16[1024,256]{1,0:T(8,128)(2,1)S(1)}, u32[]{:S(2)}, u32[]{:S(2)}) collective-permute-start(bf16[1024,256]{1,0:T(8,128)(2,1)} %collective-permute-done.8.before), channel_id=1, source_target_pairs={{0,16},{16,32},{32,48},{48,0},{1,17},{17,33},{33,49},{49,1},{2,18}... | collective-permute-start | bytes 1572872 | tf_op jit(solution)/shard_map/ppermute | solution.py:113
  133.9 13.1 %all-to-all-start.6 = ((bf16[4,72,1024]{2,1,0:T(8,128)(2,1)}), bf16[4,72,1024]{2,1,0:T(8,128)(2,1)S(1)}, u32[]{:S(2)}, u32[]{:S(2)}) async-start(bf16[4,72,1024]{2,1,0:T(8,128)(2,1)} %broadcast_in_dim.37), calls=%async_computation.6 | async-start | bytes 1179648 | tf_op jit(solution)/shard_map/all_to_all | solution.py:24
  149.3 31.9 %copy-start.14 = (f32[256]{0:T(256)S(1)}, f32[256]{0:T(256)}, u32[]{:S(2)}) copy-start(f32[256]{0:T(256)} %param.31) | copy-start | bytes 3076
  149.3 1.6 collective-permute-start.10
  151.7 15.8 %all-to-all-start.7 = ((bf16[8,16,1024]{2,1,0:T(8,128)(2,1)}), bf16[8,16,1024]{2,1,0:T(8,128)(2,1)S(1)}, u32[]{:S(2)}, u32[]{:S(2)}) async-start(bf16[8,16,1024]{2,1,0:T(8,128)(2,1)} %bitcast.31), calls=%async_computation.7 | async-start | bytes 524288 | tf_op jit(solution)/shard_map/all_to_all | solution.py:41
  (4 other events, 3.9 us)
where the time goes:
time: 184 us; the launch traced here: 182 us
  waiting for transfers between devices  73.2 us (40%)
  starting transfers between devices  52.4 us (28%)
  blocking collectives  17.2 us (9%)
  Pallas kernels  14 us (8%)
  local copies, waits for them, and re-layouts  10.1 us (5%)
  matrix products  7.8 us (4%)
  other arithmetic  6.57 us (4%)
    all_to_all x3, starting transfers between devices, copy_for_each(): lax.all_to_all(jnp.broadcast_to(x[None], (peers, *x.shape)), axis, 0, 0,...  15.4 us
    all_to_all x3, waiting for transfers between devices, copy_for_each(): lax.all_to_all(jnp.broadcast_to(x[None], (peers, *x.shape)), axis, 0, 0,...  15 us
    all_to_all x2, waiting for transfers between devices, scatter_tp(): parts = lax.all_to_all(pair.reshape(8, -1, n), 'z', 0, 0, tiled=True)  14.2 us
    all_to_all x1, waiting for transfers between devices, per_device(): lax.all_to_all(partial.reshape(16, 64, 512), KV_ROWS, 0, 0, tiled=True)  14 us
    all_to_all x1, blocking collectives, per_device(): lax.all_to_all(to_peers(jnp.concatenate([pieces, sums_sent], 2)), KV_ROWS...  12.8 us
    ppermute x3, waiting for transfers between devices, x_slots(): far = lax.ppermute(before, X, forward)  11.5 us
    ppermute x3, waiting for transfers between devices, x_slots(): before = lax.ppermute(x, X, forward)  9.09 us
    all_to_all x1, starting transfers between devices, per_device(): lax.all_to_all(partial.reshape(16, 64, 512), KV_ROWS, 0, 0, tiled=True)  7.48 us
  transfers between devices with their start and end apart: 19, of which 14 were waited for; matrix products, arithmetic and copies ran while one was open for 7% of the time, Pallas kernels for 4%

commit v1 on v0

--- a/solution.py
+++ b/solution.py
@@ -66,7 +66,7 @@
     return x.swapaxes(0, 1).reshape(4, *rest)
 
 
-def copied(kernel, out_shape, copies, *args):
+def copied(kernel, out_shape, copies, limit, *args):
     many = isinstance(out_shape, tuple)
     vmem = pl.BlockSpec(memory_space=pltpu.VMEM)
     return pl.pallas_call(
@@ -75,6 +75,7 @@
         in_specs=[pl.BlockSpec(memory_space=pl.ANY)] * len(args),
         out_specs=(vmem,) * len(out_shape) if many else vmem,
         scratch_shapes=[pltpu.SemaphoreType.DMA((copies,))],
+        compiler_params=pltpu.CompilerParams(vmem_limit_bytes=limit),
     )(*args)
 
 
@@ -105,12 +106,12 @@
         gain[:, lanes] = p[128:131].astype(F32).sum(0, keepdims=True)
 
 
-def x_slots(x):
+def x_slots(x, far_back=False):
     forward = [(i, (i + 1) % 4) for i in range(4)]
     back = [(i, (i + 3) % 4) for i in range(4)]
     before = lax.ppermute(x, X, forward)
     after = lax.ppermute(x, X, back)
-    far = lax.ppermute(before, X, forward)
+    far = lax.ppermute(after, X, back) if far_back else lax.ppermute(before, X, forward)
     return x, after, far, before
 
 
@@ -119,93 +120,73 @@
     return jnp.where(lax.broadcasted_iota(jnp.int32, x.shape, 1) < HDIM, *sums)
 
 
-def retain_kernel(
-    came, cosine, sine, offset, rate, gain, swap, ones, tokens, keys, values, state, sent
-):
+def retain_kernel(came, angles, heads, matrices, tokens, keys, values, state, sent):
+    cosine, sine, offset = [angles[:, 128 * i : 128 * i + 128] for i in range(3)]
+    rate, gain = heads[0:1], heads[1:2]
+    swap, ones = matrices[:128], matrices[128:]
+
     summed = came[...].astype(F32).sum(0).astype(BF16)
     query, keyed, valued, gated = [summed[:, 128 * i : 128 * i + 128] for i in range(4)]
 
     def rotated(u):
-        swapped = jnp.dot(u, swap[...], preferred_element_type=F32)
-        return u.astype(F32) * cosine[...] + swapped * sine[...]
-
-    q_rot = rotated(query).astype(BF16).astype(F32)
+        swapped = jnp.dot(u, swap, preferred_element_type=F32)
+        return u.astype(F32) * cosine + swapped * sine
+
+    q_short = rotated(query).astype(BF16)
+    q_rot = q_short.astype(F32)
     k_rot = (rotated(keyed) * 0.125).astype(BF16).astype(F32)
     own = head_sum(q_rot * k_rot).astype(BF16).astype(F32)
     slot = lax.broadcasted_iota(jnp.int32, (BLK, 128), 0).astype(F32)
-    growth = jnp.exp(rate[...] * slot)
+    growth = jnp.exp(rate * slot)
     key_index = lax.broadcasted_iota(jnp.int32, (HDIM, 128), 0)
     same = key_index == lax.broadcasted_iota(jnp.int32, (HDIM, 128), 1) % HDIM
+    same = jnp.where(same, 1.0, 0.0).astype(BF16)
     inner, cross = [], []
-    for s in range(16):
-        row = q_rot[s : s + 1]
-        terms = jnp.concatenate(
-            [(keys[s].astype(F32) * row).astype(BF16), jnp.where(same, row, 0.0).astype(BF16)]
-        )
-        spread = jnp.dot(terms, ones[...], preferred_element_type=F32)
+    for s in range(64):
+        row = q_short[s : s + 1]
+        terms = jnp.concatenate([keys[s] * row, same * row])
+        spread = jnp.dot(terms, ones, preferred_element_type=F32)
         weights = jnp.where(slot < offset[s : s + 1], spread[:BLK] * growth, 0.0)
         inner.append((weights * values[s].astype(F32)).sum(0, keepdims=True))
         cross.append((spread[BLK:] * state[s]).sum(0, keepdims=True))
-    inner = jnp.concatenate(inner) * jnp.exp(-rate[...] * offset[...])
-    cross = jnp.concatenate(cross) * jnp.exp(-rate[...] * (offset[...] + 1.0))
+    inner = jnp.concatenate(inner) * jnp.exp(-rate * offset)
+    cross = jnp.concatenate(cross) * jnp.exp(-rate * (offset + 1.0))
     retained = inner + own * valued.astype(F32) + cross
     centred = retained - head_sum(retained) / HDIM
     variance = head_sum(centred * centred) / HDIM
-    normed = centred * lax.rsqrt(variance + EPS) * gain[...]
+    normed = centred * lax.rsqrt(variance + EPS) * gain
     mixed = (jax.nn.silu(gated.astype(F32)) * normed).astype(BF16)
-    for y in range(4):
-        sent[0, y, 0, :, :128] = mixed
-        sent[0, y, 0, :, 128:] = tokens[...]
+    for x in range(4):
+        rows = pl.ds(16 * x, 16)
+        for y in range(4):
+            sent[x % 2, y, x // 2, :, :128] = mixed[16 * x : 16 * x + 16]
+            sent[x % 2, y, x // 2, :, 128:] = tokens[rows]
 
 
 def retain(came, lengths, state, keys, values, rate, gain, tokens):
-    lane = jnp.arange(128)
+    lane = jnp.arange(384)
     inverse = 10000.0 ** (-(lane % 32).astype(F32) / 32)
     angle = lengths.astype(F32)[:, None] * inverse[None]
     sine = jnp.sin(angle) * jnp.where(lane % HDIM < 32, -1.0, 1.0)[None]
+    offset = (lengths % BLK).astype(F32)[:, None]
+    angles = jnp.where(lane < 128, jnp.cos(angle), jnp.where(lane < 256, sine, offset))
+    lane = lane[:128]
     swap = (lane[:, None] == (lane ^ 32)[None]).astype(BF16)
     ones = (lane[:, None] // HDIM == lane[None] // HDIM).astype(BF16)
-    offset = jnp.broadcast_to((lengths % BLK).astype(F32)[:, None], (64, 128))
-
-    def rows(*rest):
-        return pl.BlockSpec((16, *rest), lambda i: (i,) + (0,) * len(rest))
-
-    def whole(*shape):
-        return pl.BlockSpec(shape, lambda i: (0,) * len(shape))
-
+    arrays = (
+        came,
+        angles,
+        jnp.stack([jnp.repeat(rate, HDIM), gain]),
+        jnp.concatenate([swap, ones]),
+        tokens,
+    )
     sent = pl.pallas_call(
         retain_kernel,
-        grid=(4,),
         out_shape=jax.ShapeDtypeStruct((2, 4, 2, 16, 384), BF16),
-        in_specs=[
-            pl.BlockSpec((16, 16, 512), lambda i: (0, i, 0)),
-            rows(128),
-            rows(128),
-            rows(128),
-            whole(1, 128),
-            whole(1, 128),
-            whole(128, 128),
-            whole(128, 128),
-            rows(256),
-            rows(BLK, 128),
-            rows(BLK, 128),
-            rows(HDIM, 128),
-        ],
-        out_specs=pl.BlockSpec((1, 4, 1, 16, 384), lambda i: (i % 2, 0, i // 2, 0, 0)),
-    )(
-        came,
-        jnp.cos(angle),
-        sine,
-        offset,
-        jnp.repeat(rate, HDIM)[None],
-        gain[None],
-        swap,
-        ones,
-        tokens,
-        keys,
-        values,
-        state,
-    )
+        in_specs=[pl.BlockSpec(memory_space=pltpu.VMEM)] * 8,
+        out_specs=pl.BlockSpec(memory_space=pltpu.VMEM),
+        compiler_params=pltpu.CompilerParams(vmem_limit_bytes=20 * 2**20),
+    )(*arrays, keys, values, state)
     return sent.reshape(16, 16, 384)
 
 
@@ -227,7 +208,9 @@
     down_weight,
     final_gain,
 ):
-    joined = jnp.concatenate([query_weight, key_weight, value_weight, gate_weight], 1)
+    joined = lax.optimization_barrier(
+        jnp.concatenate([query_weight, key_weight, value_weight, gate_weight], 1)
+    )
     all_rows = gather_tp(tokens)
     partial = jnp.dot(all_rows, joined, preferred_element_type=F32).astype(BF16)
     came = lax.all_to_all(partial.reshape(16, 64, 512), KV_ROWS, 0, 0, tiled=True)
@@ -248,13 +231,14 @@
     out_rel, gain_rel = pl.pallas_call(
         out_kernel,
         out_shape=(jax.ShapeDtypeStruct((128, 1024), BF16), jax.ShapeDtypeStruct((1, 1024), F32)),
+        compiler_params=pltpu.CompilerParams(vmem_limit_bytes=4 * 2**20),
     )(*out_slots)
     gain_rel = gain_rel[0]
     square = jax.ShapeDtypeStruct((1024, 1024), BF16)
     up_slots = x_slots(up_weight)
-    up_rel = copied(stack_kernel, square, 4, *up_slots)
-    down_slots = x_slots(down_weight)
-    down_rel = copied(beside_kernel, square, 4, *down_slots)
+    up_rel = copied(stack_kernel, square, 4, None, *up_slots)
+    down_slots = x_slots(down_weight, far_back=True)
+    down_rel = copied(beside_kernel, square, 4, None, *down_slots)
     place = lax.axis_index(X)
 
     came = lax.all_to_all(sent, KV_ROWS, 0, 0, tiled=True)
@@ -282,8 +266,12 @@
     )
     product = jnp.dot(all_gained, up_rel, preferred_element_type=F32).astype(BF16)
     sent = jnp.concatenate([product.reshape(4, 64, 1024), extra], 1)
-    came = lax.all_to_all(sent, "y", 0, 0, tiled=True)
-    total = came.astype(F32).sum(0)
+    here = lax.axis_index("y")
+    total = lax.dynamic_index_in_dim(sent, here, 0, keepdims=False).astype(F32)
+    for d in (2, 1, 3):
+        piece = lax.dynamic_index_in_dim(sent, (here + d) % 4, 0, keepdims=False)
+        came = lax.ppermute(piece, "y", [(i, (i + d) % 4) for i in range(4)])
+        total = total + came.astype(F32)
     sums = total[65, :384].reshape(3, 2, 64).sum(0)
     mean = sums[0] / 4096
     inverse = lax.rsqrt(sums[1] / 4096 - mean * mean + EPS)
@@ -293,7 +281,11 @@
     block = jnp.concatenate(
         [active, jnp.pad(stat_parts, ((0, 7), (0, 640)))]
     )
-    came = copy_for_each(block, "y")
+    came = jnp.zeros((4, 72, 1024), BF16)
+    came = lax.dynamic_update_index_in_dim(came, block, here, 0)
+    for d in (2, 1, 3):
+        piece = lax.ppermute(block, "y", [(i, (i + d) % 4) for i in range(4)])
+        came = lax.dynamic_update_index_in_dim(came, piece, (here - d) % 4, 0)
     downward = scatter_tp(
         jnp.dot(came[:, :64].reshape(256, 1024), down_rel, preferred_element_type=F32)
     )

time: 184 us -> 181 us (0.984)
  starting transfers between devices: 52.4 us -> 58.4 us
  Pallas kernels: 14 us -> 8.59 us
  waiting for transfers between devices: 73.2 us -> 68.4 us
  matrix products: 7.8 us -> 4.33 us
  blocking collectives: 17.2 us -> 20.4 us
  local copies, waits for them, and re-layouts: 10.1 us -> 12 us
    ppermute x3 -> x9, starting transfers between devices: 1.46 us -> 16.2 us  [the longest x3 6.29 us: per_device(): came = lax.ppermute(piece, 'y', [(i, (i + d) % 4) for i in range(4)])]
    ppermute x3, waiting for transfers between devices: 9.09 us -> 16.6 us  [x_slots(): before = lax.ppermute(x, X, forward)]
    all_to_all x1 -> x0, waiting for transfers between devices: 7.24 us -> none  [per_device(): came = lax.all_to_all(sent, 'y', 0, 0, tiled=True)]
    all_to_all x3 -> x2, waiting for transfers between devices: 15 us -> 9.42 us  [copy_for_each(): lax.all_to_all(jnp.broadcast_to(x[None], (peers, *x.shape)), axis, 0, 0,...]
    all_to_all x1 -> x0, starting transfers between devices: 4.24 us -> none  [per_device(): came = lax.all_to_all(sent, 'y', 0, 0, tiled=True)]
    unnamed x38 -> x36, local copies, waits for them, and re-layouts: 1.99 us -> 5.9 us
    pallas_call x1, Pallas kernels: 6.59 us -> 2.78 us  [retain(): pl.pallas_call(retain_kernel, out_shape=jax.ShapeDtypeStruct((2, 4, 2, 16...]
    all_to_all x3 -> x2, starting transfers between devices: 15.4 us -> 11.9 us  [copy_for_each(): lax.all_to_all(jnp.broadcast_to(x[None], (peers, *x.shape)), axis, 0, 0,...]
  transfers between devices with their start and end apart: 19 -> 23, of which waited for: 14 -> 14; matrix products, arithmetic and copies ran while one was open for 7% -> 6% of each run, Pallas kernels for 4% -> 3%
where the time goes in v1:
time: 181 us; the launch traced here: 179 us
  waiting for transfers between devices  68.4 us (38%)
  starting transfers between devices  58.4 us (32%)
  blocking collectives  20.4 us (11%)
  local copies, waits for them, and re-layouts  12 us (7%)
  Pallas kernels  8.59 us (5%)
  other arithmetic  6.46 us (4%)
  matrix products  4.33 us (2%)
    ppermute x3, waiting for transfers between devices, x_slots(): before = lax.ppermute(x, X, forward)  16.6 us
    all_to_all x1, blocking collectives, per_device(): lax.all_to_all(to_peers(jnp.concatenate([pieces, sums_sent], 2)), KV_ROWS...  15.8 us
    all_to_all x1, waiting for transfers between devices, per_device(): lax.all_to_all(partial.reshape(16, 64, 512), KV_ROWS, 0, 0, tiled=True)  15 us
    all_to_all x2, waiting for transfers between devices, scatter_tp(): parts = lax.all_to_all(pair.reshape(8, -1, n), 'z', 0, 0, tiled=True)  14.2 us
    all_to_all x2, starting transfers between devices, copy_for_each(): lax.all_to_all(jnp.broadcast_to(x[None], (peers, *x.shape)), axis, 0, 0,...  11.9 us
    all_to_all x2, waiting for transfers between devices, copy_for_each(): lax.all_to_all(jnp.broadcast_to(x[None], (peers, *x.shape)), axis, 0, 0,...  9.42 us
    all_to_all x1, starting transfers between devices, per_device(): lax.all_to_all(partial.reshape(16, 64, 512), KV_ROWS, 0, 0, tiled=True)  7.48 us
    ppermute x3, starting transfers between devices, x_slots(): after = lax.ppermute(x, X, back)  7.19 us
  transfers between devices with their start and end apart: 23, of which 14 were waited for; matrix products, arithmetic and copies ran while one was open for 6% of the time, Pallas kernels for 3%

profile of v1, /device:TPU:2, one launch (start us, length us, event | category | flops | bytes accessed | tf_op | source)
XLA Modules:
  0.0 179.2 jit_solution(11080815993502479617)
XLA Ops:
  1.5 8.5 %all-to-all-start = ((bf16[8,64,256]{2,1,0:T(8,128)(2,1)}), bf16[8,64,256]{2,1,0:T(8,128)(2,1)S(1)}, u32[]{:S(2)}, u32[]{:S(2)}) async-start(bf16[8,64,256]{2,1,0:T(8,128)(2,1)} %broadcast_in_dim.90), calls=%async_computation | async-start | bytes 524288 | tf_op jit(solution)/shard_map/all_to_all | solution.py:24
  12.4 9.4 %all-to-all-done = bf16[8,64,256]{2,1,0:T(8,128)(2,1)S(1)} async-done(((bf16[8,64,256]{2,1,0:T(8,128)(2,1)}), bf16[8,64,256]{2,1,0:T(8,128)(2,1)S(1)}, u32[]{:S(2)}, u32[]{:S(2)}) %all-to-all-start) | async-done | bytes 262176 | tf_op jit(solution)/shard_map/all_to_all | solution.py:24
  21.8 2.2 %all-gather = bf16[16,64,256]{2,1,0:T(8,128)(2,1)S(1)} all-gather(bf16[8,64,256]{2,1,0:T(8,128)(2,1)S(1)} %all-to-all-done), channel_id=2, replica_groups=mesh['y'=4,'xh'=2,'xl'=2,'z'=8,'c'=2] {'c'}, dimensions={0}, use_global_device_ids=true | all-gather | bytes 786432 | tf_op jit(solution)/shard_map/all_gather | solution.py:29
  25.9 7.5 %all-to-all-start.1 = ((bf16[16,64,512]{2,1,0:T(8,128)(2,1)}), bf16[16,64,512]{2,1,0:T(8,128)(2,1)S(1)}, u32[]{:S(2)}, u32[]{:S(2)}) async-start(bf16[16,64,512]{2,1,0:T(8,128)(2,1)} %bitcast.137), calls=%async_computation.1 | async-start | bytes 2097152 | tf_op jit(solution)/shard_map/all_to_all | solution.py:216
  34.0 15.0 %all-to-all-done.1.came = bf16[16,64,512]{2,1,0:T(8,128)(2,1)S(1)} async-done(((bf16[16,64,512]{2,1,0:T(8,128)(2,1)}), bf16[16,64,512]{2,1,0:T(8,128)(2,1)S(1)}, u32[]{:S(2)}, u32[]{:S(2)}) %all-to-all-start.1) | async-done | bytes 1048608 | tf_op jit(solution)/shard_map/all_to_all | solution.py:216
  49.0 1.6 copy-done.1
  50.6 1.6 copy-done.2
  52.1 2.8 %shard_map.154 = bf16[2,4,2,16,384]{4,3,2,1,0:T(8,128)(2,1)} custom-call(bf16[16,64,512]{2,1,0:T(8,128)(2,1)S(1)} %all-to-all-done.1.came, f32[64,384]{1,0:T(8,128)S(1)} %fusion.22.angles, f32[2,128]{1,0:T(2,128)S(1)} %pad_maximum_fusion.5.heads, bf16[256,128]{1,0:T(8,128)(2,1)S(1)} %add_convert_fusion.matrices, bf16[64,256]{1,0:T(8,128)(2,1)S(1)} %copy-done.3, ...), custom_call_target="tpu_custom_call" | custom-call | tf_op jit(solution)/shard_map/pallas_call | solution.py:183
  54.9 6.0 %all-to-all-start.2 = ((bf16[16,16,384]{2,1,0:T(8,128)(2,1)}), bf16[16,16,384]{2,1,0:T(8,128)(2,1)S(1)}, u32[]{:S(2)}, u32[]{:S(2)}) async-start(bf16[16,16,384]{2,1,0:T(8,128)(2,1)} %bitcast.4), calls=%async_computation.2 | async-start | bytes 393216 | tf_op jit(solution)/shard_map/all_to_all | solution.py:244
  63.2 2.3 %collective-permute-done.1.before = bf16[136,256]{1,0:T(8,128)(2,1)S(1)} collective-permute-done((bf16[136,256]{1,0:T(8,128)(2,1)S(1)}, bf16[136,256]{1,0:T(8,128)(2,1)S(1)}, u32[]{:S(2)}, u32[]{:S(2)}) %collective-permute-start.1) | collective-permute-done | bytes 69664 | tf_op jit(solution)/shard_map/ppermute | solution.py:112
  67.2 3.1 %collective-permute-done.2.far = bf16[136,256]{1,0:T(8,128)(2,1)S(1)} collective-permute-done((bf16[136,256]{1,0:T(8,128)(2,1)S(1)}, bf16[136,256]{1,0:T(8,128)(2,1)S(1)}, u32[]{:S(2)}, u32[]{:S(2)}) %collective-permute-start.2) | collective-permute-done | bytes 69664 | tf_op jit(solution)/shard_map/ppermute | solution.py:114
  73.0 3.4 %all-to-all-start.3 = ((bf16[8,16,1024]{2,1,0:T(8,128)(2,1)}), bf16[8,16,1024]{2,1,0:T(8,128)(2,1)S(1)}, u32[]{:S(2)}, u32[]{:S(2)}) async-start(bf16[8,16,1024]{2,1,0:T(8,128)(2,1)} %bitcast.14), calls=%async_computation.3 | async-start | bytes 524288 | tf_op jit(solution)/shard_map/all_to_all | solution.py:41
  76.4 3.3 %collective-permute-start.4 = (bf16[256,1024]{1,0:T(8,128)(2,1)S(1)}, bf16[256,1024]{1,0:T(8,128)(2,1)S(1)}, u32[]{:S(2)}, u32[]{:S(2)}) collective-permute-start(bf16[256,1024]{1,0:T(8,128)(2,1)S(1)} %copy-done.6), channel_id=1, source_target_pairs={{0,48},{16,0},{32,16},{48,32},{1,49},{17,1},{33,17},{49,33},{2,50}... | collective-permute-start | bytes 1572872 | tf_op jit(solution)/shard_map/ppermute | solution.py:113
  79.8 6.8 %collective-permute-done.5.before = bf16[256,1024]{1,0:T(8,128)(2,1)S(1)} collective-permute-done((bf16[256,1024]{1,0:T(8,128)(2,1)S(1)}, bf16[256,1024]{1,0:T(8,128)(2,1)S(1)}, u32[]{:S(2)}, u32[]{:S(2)}) %collective-permute-start.5) | collective-permute-done | bytes 524320 | tf_op jit(solution)/shard_map/ppermute | solution.py:112
  86.7 2.1 %all-to-all-done.3 = bf16[8,16,1024]{2,1,0:T(8,128)(2,1)S(1)} async-done(((bf16[8,16,1024]{2,1,0:T(8,128)(2,1)}), bf16[8,16,1024]{2,1,0:T(8,128)(2,1)S(1)}, u32[]{:S(2)}, u32[]{:S(2)}) %all-to-all-start.3) | async-done | bytes 262176 | tf_op jit(solution)/shard_map/all_to_all | solution.py:41
  89.6 3.4 %all-to-all-start.4 = ((bf16[8,16,1024]{2,1,0:T(8,128)(2,1)}), bf16[8,16,1024]{2,1,0:T(8,128)(2,1)S(1)}, u32[]{:S(2)}, u32[]{:S(2)}) async-start(bf16[8,16,1024]{2,1,0:T(8,128)(2,1)} %broadcast_in_dim.98), calls=%async_computation.4 | async-start | bytes 524288 | tf_op jit(solution)/shard_map/all_to_all | solution.py:24
  93.0 3.3 %collective-permute-start.13 = (bf16[1024,256]{1,0:T(8,128)(2,1)}, bf16[1024,256]{1,0:T(8,128)(2,1)}, u32[]{:S(2)}, u32[]{:S(2)}) collective-permute-start(bf16[1024,256]{1,0:T(8,128)(2,1)} %own.3), channel_id=1, source_target_pairs={{0,48},{16,0},{32,16},{48,32},{1,49},{17,1},{33,17},{49,33},{2,50}... | collective-permute-start | bytes 1572872 | tf_op jit(solution)/shard_map/ppermute | solution.py:113
  97.6 3.5 %collective-permute-done.6.far = bf16[256,1024]{1,0:T(8,128)(2,1)S(1)} collective-permute-done((bf16[256,1024]{1,0:T(8,128)(2,1)S(1)}, bf16[256,1024]{1,0:T(8,128)(2,1)S(1)}, u32[]{:S(2)}, u32[]{:S(2)}) %collective-permute-start.6) | collective-permute-done | bytes 524320 | tf_op jit(solution)/shard_map/ppermute | solution.py:114
  101.9 2.9 %shard_map.156 = bf16[1024,1024]{1,0:T(8,128)(2,1)} custom-call(bf16[256,1024]{1,0:T(8,128)(2,1)} %own.2, bf16[256,1024]{1,0:T(8,128)(2,1)} %copy-done.8, bf16[256,1024]{1,0:T(8,128)(2,1)} %copy-done.11, bf16[256,1024]{1,0:T(8,128)(2,1)} %copy-done.7), custom_call_target="tpu_custom_call" | custom-call | tf_op jit(solution)/shard_map/pallas_call | solution.py:72
  104.8 2.1 %convolution_reduce_fusion = bf16[1024]{0:T(1024)(128)(2,1)S(1)} fusion(bf16[1024,1024]{1,0:T(8,128)(2,1)} %shard_map.156, bf16[1,1024]{1,0:T(2,128)(2,1)S(1)} %get-tuple-element.21, bf16[1,1024]{1,0:T(2,128)(2,1)S(1)} %get-tuple-element.22, bf16[1,1024]{1,0:T(2,128)(2,1)S(1)} %get-tuple-element.23), kind=kOutput, calls=%fused_computation.9 | convolution fusion | flops 6311936 | bytes 2105344 | tf_op jit(solution)/shard_map/dot_general | solution.py:257
  107.0 2.4 %all-gather.1 = bf16[16,16,1024]{2,1,0:T(8,128)(2,1)S(1)} all-gather(bf16[8,16,1024]{2,1,0:T(8,128)(2,1)S(1)} %all-to-all-done.4), channel_id=3, replica_groups=mesh['y'=4,'xh'=2,'xl'=2,'z'=8,'c'=2] {'c'}, dimensions={0}, use_global_device_ids=true | all-gather | bytes 786432 | tf_op jit(solution)/shard_map/all_gather | solution.py:29
  110.9 3.1 %collective-permute-start.7 = (bf16[72,1024]{1,0:T(8,128)(2,1)S(1)}, bf16[72,1024]{1,0:T(8,128)(2,1)S(1)}, u32[]{:S(2)}, u32[]{:S(2)}) collective-permute-start(bf16[72,1024]{1,0:T(8,128)(2,1)S(1)} %get-tuple-element.15), channel_id=1, source_target_pairs={{0,128},{64,192},{128,0},{192,64},{1,129},{65,193},{129,1},{193,65... | collective-permute-start | bytes 442376 | tf_op jit(solution)/shard_map/ppermute | solution.py:273
  114.5 2.7 %collective-permute-start.9 = (bf16[72,1024]{1,0:T(8,128)(2,1)S(1)}, bf16[72,1024]{1,0:T(8,128)(2,1)S(1)}, u32[]{:S(2)}, u32[]{:S(2)}) collective-permute-start(bf16[72,1024]{1,0:T(8,128)(2,1)S(1)} %get-tuple-element.16), channel_id=1, source_target_pairs={{0,192},{64,0},{128,64},{192,128},{1,193},{65,1},{129,65},{193,129... | collective-permute-start | bytes 442376 | tf_op jit(solution)/shard_map/ppermute | solution.py:273
  117.2 3.0 %collective-permute-start.14 = (bf16[1024,256]{1,0:T(8,128)(2,1)}, bf16[1024,256]{1,0:T(8,128)(2,1)S(1)}, u32[]{:S(2)}, u32[]{:S(2)}) collective-permute-start(bf16[1024,256]{1,0:T(8,128)(2,1)} %collective-permute-done.13.after), channel_id=1, source_target_pairs={{0,48},{16,0},{32,16},{48,32},{1,49},{17,1},{33,17},{49,33},{2,50}... | collective-permute-start | bytes 1572872 | tf_op jit(solution)/shard_map/ppermute | solution.py:114
  122.1 2.2 %collective-permute-start.10 = (bf16[72,1024]{1,0:T(8,128)(2,1)S(1)}, bf16[72,1024]{1,0:T(8,128)(2,1)S(1)}, u32[]{:S(2)}, u32[]{:S(2)}) collective-permute-start(bf16[72,1024]{1,0:T(8,128)(2,1)S(1)} %fusion.21), channel_id=1, source_target_pairs={{0,128},{64,192},{128,0},{192,64},{1,129},{65,193},{129,1},{193,65... | collective-permute-start | bytes 442376 | tf_op jit(solution)/shard_map/ppermute | solution.py:287
  124.3 7.5 %collective-permute-done.15.before = bf16[1024,256]{1,0:T(8,128)(2,1)S(1)} collective-permute-done((bf16[1024,256]{1,0:T(8,128)(2,1)}, bf16[1024,256]{1,0:T(8,128)(2,1)S(1)}, u32[]{:S(2)}, u32[]{:S(2)}) %collective-permute-start.15) | collective-permute-done | bytes 524320 | tf_op jit(solution)/shard_map/ppermute | solution.py:112
  133.4 2.9 %shard_map.157 = bf16[1024,1024]{1,0:T(8,128)(2,1)} custom-call(bf16[1024,256]{1,0:T(8,128)(2,1)} %own.3, bf16[1024,256]{1,0:T(8,128)(2,1)} %collective-permute-done.13.after, bf16[1024,256]{1,0:T(8,128)(2,1)} %copy-done.10, bf16[1024,256]{1,0:T(8,128)(2,1)} %copy-done.9), custom_call_target="tpu_custom_call" | custom-call | tf_op jit(solution)/shard_map/pallas_call | solution.py:72
  136.4 3.2 %collective-permute-start.12 = (bf16[72,1024]{1,0:T(8,128)(2,1)S(1)}, bf16[72,1024]{1,0:T(8,128)(2,1)S(1)}, u32[]{:S(2)}, u32[]{:S(2)}) collective-permute-start(bf16[72,1024]{1,0:T(8,128)(2,1)S(1)} %fusion.21), channel_id=1, source_target_pairs={{0,192},{64,0},{128,64},{192,128},{1,193},{65,1},{129,65},{193,129... | collective-permute-start | bytes 442376 | tf_op jit(solution)/shard_map/ppermute | solution.py:287
  139.7 3.0 %collective-permute-done.11 = bf16[72,1024]{1,0:T(8,128)(2,1)S(1)} collective-permute-done((bf16[72,1024]{1,0:T(8,128)(2,1)S(1)}, bf16[72,1024]{1,0:T(8,128)(2,1)S(1)}, u32[]{:S(2)}, u32[]{:S(2)}) %collective-permute-start.11) | collective-permute-done | bytes 147488 | tf_op jit(solution)/shard_map/ppermute | solution.py:287
  146.0 3.4 %all-to-all-start.5 = ((bf16[8,16,1024]{2,1,0:T(8,128)(2,1)}), bf16[8,16,1024]{2,1,0:T(8,128)(2,1)S(1)}, u32[]{:S(2)}, u32[]{:S(2)}) async-start(bf16[8,16,1024]{2,1,0:T(8,128)(2,1)} %bitcast.39), calls=%async_computation.5 | async-start | bytes 524288 | tf_op jit(solution)/shard_map/all_to_all | solution.py:41
  149.7 12.1 %all-to-all-done.5 = bf16[8,16,1024]{2,1,0:T(8,128)(2,1)S(1)} async-done(((bf16[8,16,1024]{2,1,0:T(8,128)(2,1)}), bf16[8,16,1024]{2,1,0:T(8,128)(2,1)S(1)}, u32[]{:S(2)}, u32[]{:S(2)}) %all-to-all-start.5) | async-done | bytes 262176 | tf_op jit(solution)/shard_map/all_to_all | solution.py:41
  162.3 15.8 %all_to_all.35 = bf16[16,16,384]{2,1,0:T(8,128)(2,1)S(1)} all-to-all(bf16[16,16,384]{2,1,0:T(8,128)(2,1)S(1)} %bitcast.142), channel_id=1, replica_groups=mesh['y'=4,'xh'=2,'xl'=2,'z'=8,'c'=2] {'xl','y','xh'}, dimensions={0} | all-to-all | bytes 393216 | tf_op jit(solution)/shard_map/all_to_all | solution.py:303
  (155 shorter events, 26.7 us)
Async XLA Ops:
  1.5 20.3 %all-to-all-start = ((bf16[8,64,256]{2,1,0:T(8,128)(2,1)}), bf16[8,64,256]{2,1,0:T(8,128)(2,1)S(1)}, u32[]{:S(2)}, u32[]{:S(2)}) async-start(bf16[8,64,256]{2,1,0:T(8,128)(2,1)} %broadcast_in_dim.90), calls=%async_computation | async-start | bytes 524288 | tf_op jit(solution)/shard_map/all_to_all | solution.py:24
  24.5 9.0 %copy-start.15 = (s32[64]{0:T(128)S(1)}, s32[64]{0:T(128)}, u32[]{:S(2)}) copy-start(s32[64]{0:T(128)} %param.17) | copy-start | bytes 772
  24.5 24.4 %copy-start = (bf16[64,128,128]{2,1,0:T(8,128)(2,1)S(1)}, bf16[64,128,128]{2,1,0:T(8,128)(2,1)}, u32[]{:S(2)}) copy-start(bf16[64,128,128]{2,1,0:T(8,128)(2,1)} %keys.1) | copy-start | bytes 6291460
  24.5 24.4 %copy-start.3 = (bf16[64,256]{1,0:T(8,128)(2,1)S(1)}, bf16[64,256]{1,0:T(8,128)(2,1)}, u32[]{:S(2)}) copy-start(bf16[64,256]{1,0:T(8,128)(2,1)} %tokens.1) | copy-start | bytes 98308
  25.9 23.1 %all-to-all-start.1 = ((bf16[16,64,512]{2,1,0:T(8,128)(2,1)}), bf16[16,64,512]{2,1,0:T(8,128)(2,1)S(1)}, u32[]{:S(2)}, u32[]{:S(2)}) async-start(bf16[16,64,512]{2,1,0:T(8,128)(2,1)} %bitcast.137), calls=%async_computation.1 | async-start | bytes 2097152 | tf_op jit(solution)/shard_map/all_to_all | solution.py:216
  52.1 8.8 %copy-start.14 = (f32[256]{0:T(256)S(1)}, f32[256]{0:T(256)}, u32[]{:S(2)}) copy-start(f32[256]{0:T(256)} %param.28) | copy-start | bytes 3076
  52.1 8.9 %copy-start.12 = (bf16[128,256]{1,0:T(8,128)(2,1)S(1)}, bf16[128,256]{1,0:T(8,128)(2,1)}, u32[]{:S(2)}) copy-start(bf16[128,256]{1,0:T(8,128)(2,1)} %param.27) | copy-start | bytes 196612
  54.9 15.8 %copy-start.6 = (bf16[256,1024]{1,0:T(8,128)(2,1)S(1)}, bf16[256,1024]{1,0:T(8,128)(2,1)}, u32[]{:S(2)}) copy-start(bf16[256,1024]{1,0:T(8,128)(2,1)} %own.2) | copy-start | bytes 1572868
  54.9 15.3 %all-to-all-start.2 = ((bf16[16,16,384]{2,1,0:T(8,128)(2,1)}), bf16[16,16,384]{2,1,0:T(8,128)(2,1)S(1)}, u32[]{:S(2)}, u32[]{:S(2)}) async-start(bf16[16,16,384]{2,1,0:T(8,128)(2,1)} %bitcast.4), calls=%async_computation.2 | async-start | bytes 393216 | tf_op jit(solution)/shard_map/all_to_all | solution.py:244
  61.1 4.4 %collective-permute-start.1 = (bf16[136,256]{1,0:T(8,128)(2,1)S(1)}, bf16[136,256]{1,0:T(8,128)(2,1)S(1)}, u32[]{:S(2)}, u32[]{:S(2)}) collective-permute-start(bf16[136,256]{1,0:T(8,128)(2,1)S(1)} %concatenate.85.own), channel_id=1, source_target_pairs={{0,16},{16,32},{32,48},{48,0},{1,17},{17,33},{33,49},{49,1},{2,18}... | collective-permute-start | bytes 208904 | tf_op jit(solution)/shard_map/ppermute | solution.py:112
  62.6 4.6 %collective-permute-start = (bf16[136,256]{1,0:T(8,128)(2,1)S(1)}, bf16[136,256]{1,0:T(8,128)(2,1)S(1)}, u32[]{:S(2)}, u32[]{:S(2)}) collective-permute-start(bf16[136,256]{1,0:T(8,128)(2,1)S(1)} %concatenate.85.own), channel_id=1, source_target_pairs={{0,48},{16,0},{32,16},{48,32},{1,49},{17,1},{33,17},{49,33},{2,50}... | collective-permute-start | bytes 208904 | tf_op jit(solution)/shard_map/ppermute | solution.py:113
  65.5 4.8 %collective-permute-start.2 = (bf16[136,256]{1,0:T(8,128)(2,1)S(1)}, bf16[136,256]{1,0:T(8,128)(2,1)S(1)}, u32[]{:S(2)}, u32[]{:S(2)}) collective-permute-start(bf16[136,256]{1,0:T(8,128)(2,1)S(1)} %collective-permute-done.1.before), channel_id=1, source_target_pairs={{0,16},{16,32},{32,48},{48,0},{1,17},{17,33},{33,49},{49,1},{2,18}... | collective-permute-start | bytes 208904 | tf_op jit(solution)/shard_map/ppermute | solution.py:114
  70.6 1.6 collective-permute-start.3
  70.7 15.8 %collective-permute-start.5 = (bf16[256,1024]{1,0:T(8,128)(2,1)S(1)}, bf16[256,1024]{1,0:T(8,128)(2,1)S(1)}, u32[]{:S(2)}, u32[]{:S(2)}) collective-permute-start(bf16[256,1024]{1,0:T(8,128)(2,1)S(1)} %copy-done.6), channel_id=1, source_target_pairs={{0,16},{16,32},{32,48},{48,0},{1,17},{17,33},{33,49},{49,1},{2,18}... | collective-permute-start | bytes 1572872 | tf_op jit(solution)/shard_map/ppermute | solution.py:112
  73.0 15.8 %all-to-all-start.3 = ((bf16[8,16,1024]{2,1,0:T(8,128)(2,1)}), bf16[8,16,1024]{2,1,0:T(8,128)(2,1)S(1)}, u32[]{:S(2)}, u32[]{:S(2)}) async-start(bf16[8,16,1024]{2,1,0:T(8,128)(2,1)} %bitcast.14), calls=%async_computation.3 | async-start | bytes 524288 | tf_op jit(solution)/shard_map/all_to_all | solution.py:41
  76.4 21.2 %collective-permute-start.4 = (bf16[256,1024]{1,0:T(8,128)(2,1)S(1)}, bf16[256,1024]{1,0:T(8,128)(2,1)S(1)}, u32[]{:S(2)}, u32[]{:S(2)}) collective-permute-start(bf16[256,1024]{1,0:T(8,128)(2,1)S(1)} %copy-done.6), channel_id=1, source_target_pairs={{0,48},{16,0},{32,16},{48,32},{1,49},{17,1},{33,17},{49,33},{2,50}... | collective-permute-start | bytes 1572872 | tf_op jit(solution)/shard_map/ppermute | solution.py:113
  86.5 14.6 %copy-start.7 = (bf16[256,1024]{1,0:T(8,128)(2,1)}, bf16[256,1024]{1,0:T(8,128)(2,1)S(1)}, u32[]{:S(2)}) copy-start(bf16[256,1024]{1,0:T(8,128)(2,1)S(1)} %collective-permute-done.5.before) | copy-start | bytes 1572868
  86.6 14.6 %collective-permute-start.6 = (bf16[256,1024]{1,0:T(8,128)(2,1)S(1)}, bf16[256,1024]{1,0:T(8,128)(2,1)S(1)}, u32[]{:S(2)}, u32[]{:S(2)}) collective-permute-start(bf16[256,1024]{1,0:T(8,128)(2,1)S(1)} %collective-permute-done.5.before), channel_id=1, source_target_pairs={{0,16},{16,32},{32,48},{48,0},{1,17},{17,33},{33,49},{49,1},{2,18}... | collective-permute-start | bytes 1572872 | tf_op jit(solution)/shard_map/ppermute | solution.py:114
  89.6 17.4 %all-to-all-start.4 = ((bf16[8,16,1024]{2,1,0:T(8,128)(2,1)}), bf16[8,16,1024]{2,1,0:T(8,128)(2,1)S(1)}, u32[]{:S(2)}, u32[]{:S(2)}) async-start(bf16[8,16,1024]{2,1,0:T(8,128)(2,1)} %broadcast_in_dim.98), calls=%async_computation.4 | async-start | bytes 524288 | tf_op jit(solution)/shard_map/all_to_all | solution.py:24
  93.0 24.2 %collective-permute-start.13 = (bf16[1024,256]{1,0:T(8,128)(2,1)}, bf16[1024,256]{1,0:T(8,128)(2,1)}, u32[]{:S(2)}, u32[]{:S(2)}) collective-permute-start(bf16[1024,256]{1,0:T(8,128)(2,1)} %own.3), channel_id=1, source_target_pairs={{0,48},{16,0},{32,16},{48,32},{1,49},{17,1},{33,17},{49,33},{2,50}... | collective-permute-start | bytes 1572872 | tf_op jit(solution)/shard_map/ppermute | solution.py:113
  110.9 9.3 %collective-permute-start.7 = (bf16[72,1024]{1,0:T(8,128)(2,1)S(1)}, bf16[72,1024]{1,0:T(8,128)(2,1)S(1)}, u32[]{:S(2)}, u32[]{:S(2)}) collective-permute-start(bf16[72,1024]{1,0:T(8,128)(2,1)S(1)} %get-tuple-element.15), channel_id=1, source_target_pairs={{0,128},{64,192},{128,0},{192,64},{1,129},{65,193},{129,1},{193,65... | collective-permute-start | bytes 442376 | tf_op jit(solution)/shard_map/ppermute | solution.py:273
  114.0 7.6 %collective-permute-start.8 = (bf16[72,1024]{1,0:T(8,128)(2,1)S(1)}, bf16[72,1024]{1,0:T(8,128)(2,1)S(1)}, u32[]{:S(2)}, u32[]{:S(2)}) collective-permute-start(bf16[72,1024]{1,0:T(8,128)(2,1)S(1)} %get-tuple-element.17), channel_id=1, source_target_pairs={{0,64},{64,128},{128,192},{192,0},{1,65},{65,129},{129,193},{193,1... | collective-permute-start | bytes 442376 | tf_op jit(solution)/shard_map/ppermute | solution.py:273
  114.5 7.1 %collective-permute-start.9 = (bf16[72,1024]{1,0:T(8,128)(2,1)S(1)}, bf16[72,1024]{1,0:T(8,128)(2,1)S(1)}, u32[]{:S(2)}, u32[]{:S(2)}) collective-permute-start(bf16[72,1024]{1,0:T(8,128)(2,1)S(1)} %get-tuple-element.16), channel_id=1, source_target_pairs={{0,192},{64,0},{128,64},{192,128},{1,193},{65,1},{129,65},{193,129... | collective-permute-start | bytes 442376 | tf_op jit(solution)/shard_map/ppermute | solution.py:273
  117.2 14.5 %collective-permute-start.15 = (bf16[1024,256]{1,0:T(8,128)(2,1)}, bf16[1024,256]{1,0:T(8,128)(2,1)S(1)}, u32[]{:S(2)}, u32[]{:S(2)}) collective-permute-start(bf16[1024,256]{1,0:T(8,128)(2,1)} %own.3), channel_id=1, source_target_pairs={{0,16},{16,32},{32,48},{48,0},{1,17},{17,33},{33,49},{49,1},{2,18}... | collective-permute-start | bytes 1572872 | tf_op jit(solution)/shard_map/ppermute | solution.py:112
  117.2 14.5 %collective-permute-start.14 = (bf16[1024,256]{1,0:T(8,128)(2,1)}, bf16[1024,256]{1,0:T(8,128)(2,1)S(1)}, u32[]{:S(2)}, u32[]{:S(2)}) collective-permute-start(bf16[1024,256]{1,0:T(8,128)(2,1)} %collective-permute-done.13.after), channel_id=1, source_target_pairs={{0,48},{16,0},{32,16},{48,32},{1,49},{17,1},{33,17},{49,33},{2,50}... | collective-permute-start | bytes 1572872 | tf_op jit(solution)/shard_map/ppermute | solution.py:114
  122.1 17.6 %collective-permute-start.10 = (bf16[72,1024]{1,0:T(8,128)(2,1)S(1)}, bf16[72,1024]{1,0:T(8,128)(2,1)S(1)}, u32[]{:S(2)}, u32[]{:S(2)}) collective-permute-start(bf16[72,1024]{1,0:T(8,128)(2,1)S(1)} %fusion.21), channel_id=1, source_target_pairs={{0,128},{64,192},{128,0},{192,64},{1,129},{65,193},{129,1},{193,65... | collective-permute-start | bytes 442376 | tf_op jit(solution)/shard_map/ppermute | solution.py:287
  136.3 6.5 %copy-start.4 = (bf16[1024,1024]{1,0:T(8,128)(2,1)S(1)}, bf16[1024,1024]{1,0:T(8,128)(2,1)}, u32[]{:S(2)}) copy-start(bf16[1024,1024]{1,0:T(8,128)(2,1)} %shard_map.157) | copy-start | bytes 6291460
  136.3 6.4 %collective-permute-start.11 = (bf16[72,1024]{1,0:T(8,128)(2,1)S(1)}, bf16[72,1024]{1,0:T(8,128)(2,1)S(1)}, u32[]{:S(2)}, u32[]{:S(2)}) collective-permute-start(bf16[72,1024]{1,0:T(8,128)(2,1)S(1)} %fusion.21), channel_id=1, source_target_pairs={{0,64},{64,128},{128,192},{192,0},{1,65},{65,129},{129,193},{193,1... | collective-permute-start | bytes 442376 | tf_op jit(solution)/shard_map/ppermute | solution.py:287
  136.4 6.4 %collective-permute-start.12 = (bf16[72,1024]{1,0:T(8,128)(2,1)S(1)}, bf16[72,1024]{1,0:T(8,128)(2,1)S(1)}, u32[]{:S(2)}, u32[]{:S(2)}) collective-permute-start(bf16[72,1024]{1,0:T(8,128)(2,1)S(1)} %fusion.21), channel_id=1, source_target_pairs={{0,192},{64,0},{128,64},{192,128},{1,193},{65,1},{129,65},{193,129... | collective-permute-start | bytes 442376 | tf_op jit(solution)/shard_map/ppermute | solution.py:287
  143.6 35.0 %copy-start.13 = (f32[256]{0:T(256)S(1)}, f32[256]{0:T(256)}, u32[]{:S(2)}) copy-start(f32[256]{0:T(256)} %param.31) | copy-start | bytes 3076
  143.6 1.6 collective-permute-start.16
  146.0 15.8 %all-to-all-start.5 = ((bf16[8,16,1024]{2,1,0:T(8,128)(2,1)}), bf16[8,16,1024]{2,1,0:T(8,128)(2,1)S(1)}, u32[]{:S(2)}, u32[]{:S(2)}) async-start(bf16[8,16,1024]{2,1,0:T(8,128)(2,1)} %bitcast.39), calls=%async_computation.5 | async-start | bytes 524288 | tf_op jit(solution)/shard_map/all_to_all | solution.py:41
  (7 other events, 14.1 us)

commit v2 on v1

--- a/solution.py
+++ b/solution.py
@@ -2,6 +2,7 @@
 import jax.numpy as jnp
 from jax import lax
 from jax.experimental import pallas as pl
+from jax.experimental.layout import Layout, with_layout_constraint
 from jax.experimental.pallas import tpu as pltpu
 from jax.sharding import Mesh
 from jax.sharding import PartitionSpec as P
@@ -120,7 +121,22 @@
     return jnp.where(lax.broadcasted_iota(jnp.int32, x.shape, 1) < HDIM, *sums)
 
 
-def retain_kernel(came, angles, heads, matrices, tokens, keys, values, state, sent):
+def retain_kernel(
+    came, angles, heads, matrices, tokens, keys, values_from, state_from, sent, values, state, sems
+):
+    groups = []
+    for i in range(4):
+        rows = pl.ds(16 * i, 16)
+        pairs = ((values_from, values), (state_from, state))
+        groups.append(
+            [
+                pltpu.make_async_copy(source.at[rows], target.at[rows], sems.at[i, j])
+                for j, (source, target) in enumerate(pairs)
+            ]
+        )
+    for group in groups:
+        for copy in group:
+            copy.start()
     cosine, sine, offset = [angles[:, 128 * i : 128 * i + 128] for i in range(3)]
     rate, gain = heads[0:1], heads[1:2]
     swap, ones = matrices[:128], matrices[128:]
@@ -143,6 +159,9 @@
     same = jnp.where(same, 1.0, 0.0).astype(BF16)
     inner, cross = [], []
     for s in range(64):
+        if s % 16 == 0:
+            for copy in groups[s // 16]:
+                copy.wait()
         row = q_short[s : s + 1]
         terms = jnp.concatenate([keys[s] * row, same * row])
         spread = jnp.dot(terms, ones, preferred_element_type=F32)
@@ -183,9 +202,15 @@
     sent = pl.pallas_call(
         retain_kernel,
         out_shape=jax.ShapeDtypeStruct((2, 4, 2, 16, 384), BF16),
-        in_specs=[pl.BlockSpec(memory_space=pltpu.VMEM)] * 8,
+        in_specs=[pl.BlockSpec(memory_space=pltpu.VMEM)] * 6
+        + [pl.BlockSpec(memory_space=pl.ANY)] * 2,
         out_specs=pl.BlockSpec(memory_space=pltpu.VMEM),
-        compiler_params=pltpu.CompilerParams(vmem_limit_bytes=20 * 2**20),
+        scratch_shapes=[
+            pltpu.VMEM((64, BLK, 128), BF16),
+            pltpu.VMEM((64, HDIM, 128), F32),
+            pltpu.SemaphoreType.DMA((4, 2)),
+        ],
+        compiler_params=pltpu.CompilerParams(vmem_limit_bytes=52000000),
     )(*arrays, keys, values, state)
     return sent.reshape(16, 16, 384)
 
@@ -213,6 +238,7 @@
     )
     all_rows = gather_tp(tokens)
     partial = jnp.dot(all_rows, joined, preferred_element_type=F32).astype(BF16)
+    partial = with_layout_constraint(partial, Layout((0, 1)))
     came = lax.all_to_all(partial.reshape(16, 64, 512), KV_ROWS, 0, 0, tiled=True)
     sent = retain(
         came,

time: 181 us -> 179 us (0.989)
  local copies, waits for them, and re-layouts: 12 us -> 7.5 us
    unnamed x36 -> x32, local copies, waits for them, and re-layouts: 5.9 us -> 2.72 us
where the time goes in v2:
time: 179 us; the launch traced here: 177 us
  waiting for transfers between devices  68.4 us (38%)
  starting transfers between devices  58.4 us (33%)
  blocking collectives  20.4 us (11%)
  Pallas kernels  10.2 us (6%)
  local copies, waits for them, and re-layouts  7.5 us (4%)
  other arithmetic  6.43 us (4%)
  matrix products  5.28 us (3%)
    ppermute x3, waiting for transfers between devices, x_slots(): before = lax.ppermute(x, X, forward)  16.6 us
    all_to_all x1, blocking collectives, per_device(): lax.all_to_all(to_peers(jnp.concatenate([pieces, sums_sent], 2)), KV_ROWS...  15.9 us
    all_to_all x1, waiting for transfers between devices, per_device(): lax.all_to_all(partial.reshape(16, 64, 512), KV_ROWS, 0, 0, tiled=True)  14.9 us
    all_to_all x2, waiting for transfers between devices, scatter_tp(): parts = lax.all_to_all(pair.reshape(8, -1, n), 'z', 0, 0, tiled=True)  14.2 us
    all_to_all x2, starting transfers between devices, copy_for_each(): lax.all_to_all(jnp.broadcast_to(x[None], (peers, *x.shape)), axis, 0, 0,...  11.9 us
    all_to_all x2, waiting for transfers between devices, copy_for_each(): lax.all_to_all(jnp.broadcast_to(x[None], (peers, *x.shape)), axis, 0, 0,...  9.42 us
    all_to_all x1, starting transfers between devices, per_device(): lax.all_to_all(partial.reshape(16, 64, 512), KV_ROWS, 0, 0, tiled=True)  7.48 us
    ppermute x3, starting transfers between devices, x_slots(): after = lax.ppermute(x, X, back)  7.19 us
  transfers between devices with their start and end apart: 23, of which 14 were waited for; matrix products, arithmetic and copies ran while one was open for 6% of the time, Pallas kernels for 3%

profile of v2, /device:TPU:2, one launch (start us, length us, event | category | flops | bytes accessed | tf_op | source)
XLA Modules:
  0.0 177.2 jit_solution(9434998907829046894)
XLA Ops:
  1.5 8.5 %all-to-all-start = ((bf16[8,64,256]{2,1,0:T(8,128)(2,1)}), bf16[8,64,256]{2,1,0:T(8,128)(2,1)S(1)}, u32[]{:S(2)}, u32[]{:S(2)}) async-start(bf16[8,64,256]{2,1,0:T(8,128)(2,1)} %broadcast_in_dim.90), calls=%async_computation | async-start | bytes 524288 | tf_op jit(solution)/shard_map/all_to_all | solution.py:25
  12.4 9.4 %all-to-all-done = bf16[8,64,256]{2,1,0:T(8,128)(2,1)S(1)} async-done(((bf16[8,64,256]{2,1,0:T(8,128)(2,1)}), bf16[8,64,256]{2,1,0:T(8,128)(2,1)S(1)}, u32[]{:S(2)}, u32[]{:S(2)}) %all-to-all-start) | async-done | bytes 262176 | tf_op jit(solution)/shard_map/all_to_all | solution.py:25
  21.8 2.2 %all-gather = bf16[16,64,256]{2,1,0:T(8,128)(2,1)S(1)} all-gather(bf16[8,64,256]{2,1,0:T(8,128)(2,1)S(1)} %all-to-all-done), channel_id=2, replica_groups=mesh['y'=4,'xh'=2,'xl'=2,'z'=8,'c'=2] {'c'}, dimensions={0}, use_global_device_ids=true | all-gather | bytes 786432 | tf_op jit(solution)/shard_map/all_gather | solution.py:30
  25.4 7.5 %all-to-all-start.1 = ((bf16[16,64,512]{2,1,0:T(8,128)(2,1)}), bf16[16,64,512]{2,1,0:T(8,128)(2,1)S(1)}, u32[]{:S(2)}, u32[]{:S(2)}) async-start(bf16[16,64,512]{2,1,0:T(8,128)(2,1)} %bitcast.137), calls=%async_computation.1 | async-start | bytes 2097152 | tf_op jit(solution)/shard_map/all_to_all | solution.py:242
  33.6 14.9 %all-to-all-done.1.came = bf16[16,64,512]{2,1,0:T(8,128)(2,1)S(1)} async-done(((bf16[16,64,512]{2,1,0:T(8,128)(2,1)}), bf16[16,64,512]{2,1,0:T(8,128)(2,1)S(1)}, u32[]{:S(2)}, u32[]{:S(2)}) %all-to-all-start.1) | async-done | bytes 1048608 | tf_op jit(solution)/shard_map/all_to_all | solution.py:242
  48.5 4.4 %shard_map.154 = bf16[2,4,2,16,384]{4,3,2,1,0:T(8,128)(2,1)} custom-call(bf16[16,64,512]{2,1,0:T(8,128)(2,1)S(1)} %all-to-all-done.1.came, f32[64,384]{1,0:T(8,128)S(1)} %fusion.21.angles, f32[2,128]{1,0:T(2,128)S(1)} %pad_maximum_fusion.5.heads, bf16[256,128]{1,0:T(8,128)(2,1)S(1)} %add_convert_fusion.matrices, bf16[64,256]{1,0:T(8,128)(2,1)S(1)} %copy-done.1, ...), custom_call_target="tpu_custom_call" | custom-call | tf_op jit(solution)/shard_map/pallas_call | solution.py:202
  52.9 6.1 %all-to-all-start.2 = ((bf16[16,16,384]{2,1,0:T(8,128)(2,1)}), bf16[16,16,384]{2,1,0:T(8,128)(2,1)S(1)}, u32[]{:S(2)}, u32[]{:S(2)}) async-start(bf16[16,16,384]{2,1,0:T(8,128)(2,1)} %bitcast.4), calls=%async_computation.2 | async-start | bytes 393216 | tf_op jit(solution)/shard_map/all_to_all | solution.py:270
  59.1 1.5 collective-permute-start.1
  61.2 2.3 %collective-permute-done.1.before = bf16[136,256]{1,0:T(8,128)(2,1)S(1)} collective-permute-done((bf16[136,256]{1,0:T(8,128)(2,1)S(1)}, bf16[136,256]{1,0:T(8,128)(2,1)S(1)}, u32[]{:S(2)}, u32[]{:S(2)}) %collective-permute-start.1) | collective-permute-done | bytes 69664 | tf_op jit(solution)/shard_map/ppermute | solution.py:113
  65.1 3.1 %collective-permute-done.2.far = bf16[136,256]{1,0:T(8,128)(2,1)S(1)} collective-permute-done((bf16[136,256]{1,0:T(8,128)(2,1)S(1)}, bf16[136,256]{1,0:T(8,128)(2,1)S(1)}, u32[]{:S(2)}, u32[]{:S(2)}) %collective-permute-start.2) | collective-permute-done | bytes 69664 | tf_op jit(solution)/shard_map/ppermute | solution.py:115
  71.0 3.4 %all-to-all-start.3 = ((bf16[8,16,1024]{2,1,0:T(8,128)(2,1)}), bf16[8,16,1024]{2,1,0:T(8,128)(2,1)S(1)}, u32[]{:S(2)}, u32[]{:S(2)}) async-start(bf16[8,16,1024]{2,1,0:T(8,128)(2,1)} %bitcast.14), calls=%async_computation.3 | async-start | bytes 524288 | tf_op jit(solution)/shard_map/all_to_all | solution.py:42
  74.4 3.3 %collective-permute-start.4 = (bf16[256,1024]{1,0:T(8,128)(2,1)S(1)}, bf16[256,1024]{1,0:T(8,128)(2,1)S(1)}, u32[]{:S(2)}, u32[]{:S(2)}) collective-permute-start(bf16[256,1024]{1,0:T(8,128)(2,1)S(1)} %copy-done.4), channel_id=1, source_target_pairs={{0,48},{16,0},{32,16},{48,32},{1,49},{17,1},{33,17},{49,33},{2,50}... | collective-permute-start | bytes 1572872 | tf_op jit(solution)/shard_map/ppermute | solution.py:114
  77.7 6.8 %collective-permute-done.5.before = bf16[256,1024]{1,0:T(8,128)(2,1)S(1)} collective-permute-done((bf16[256,1024]{1,0:T(8,128)(2,1)S(1)}, bf16[256,1024]{1,0:T(8,128)(2,1)S(1)}, u32[]{:S(2)}, u32[]{:S(2)}) %collective-permute-start.5) | collective-permute-done | bytes 524320 | tf_op jit(solution)/shard_map/ppermute | solution.py:113
  84.6 2.1 %all-to-all-done.3 = bf16[8,16,1024]{2,1,0:T(8,128)(2,1)S(1)} async-done(((bf16[8,16,1024]{2,1,0:T(8,128)(2,1)}), bf16[8,16,1024]{2,1,0:T(8,128)(2,1)S(1)}, u32[]{:S(2)}, u32[]{:S(2)}) %all-to-all-start.3) | async-done | bytes 262176 | tf_op jit(solution)/shard_map/all_to_all | solution.py:42
  87.6 3.4 %all-to-all-start.4 = ((bf16[8,16,1024]{2,1,0:T(8,128)(2,1)}), bf16[8,16,1024]{2,1,0:T(8,128)(2,1)S(1)}, u32[]{:S(2)}, u32[]{:S(2)}) async-start(bf16[8,16,1024]{2,1,0:T(8,128)(2,1)} %broadcast_in_dim.98), calls=%async_computation.4 | async-start | bytes 524288 | tf_op jit(solution)/shard_map/all_to_all | solution.py:25
  91.0 3.3 %collective-permute-start.13 = (bf16[1024,256]{1,0:T(8,128)(2,1)}, bf16[1024,256]{1,0:T(8,128)(2,1)}, u32[]{:S(2)}, u32[]{:S(2)}) collective-permute-start(bf16[1024,256]{1,0:T(8,128)(2,1)} %own.3), channel_id=1, source_target_pairs={{0,48},{16,0},{32,16},{48,32},{1,49},{17,1},{33,17},{49,33},{2,50}... | collective-permute-start | bytes 1572872 | tf_op jit(solution)/shard_map/ppermute | solution.py:114
  95.6 3.5 %collective-permute-done.6.far = bf16[256,1024]{1,0:T(8,128)(2,1)S(1)} collective-permute-done((bf16[256,1024]{1,0:T(8,128)(2,1)S(1)}, bf16[256,1024]{1,0:T(8,128)(2,1)S(1)}, u32[]{:S(2)}, u32[]{:S(2)}) %collective-permute-start.6) | collective-permute-done | bytes 524320 | tf_op jit(solution)/shard_map/ppermute | solution.py:115
  99.9 2.9 %shard_map.156 = bf16[1024,1024]{1,0:T(8,128)(2,1)} custom-call(bf16[256,1024]{1,0:T(8,128)(2,1)} %own.2, bf16[256,1024]{1,0:T(8,128)(2,1)} %copy-done.6, bf16[256,1024]{1,0:T(8,128)(2,1)} %copy-done.9, bf16[256,1024]{1,0:T(8,128)(2,1)} %copy-done.5), custom_call_target="tpu_custom_call" | custom-call | tf_op jit(solution)/shard_map/pallas_call | solution.py:73
  102.8 2.1 %convolution_reduce_fusion = bf16[1024]{0:T(1024)(128)(2,1)S(1)} fusion(bf16[1024,1024]{1,0:T(8,128)(2,1)} %shard_map.156, bf16[1,1024]{1,0:T(2,128)(2,1)S(1)} %get-tuple-element.21, bf16[1,1024]{1,0:T(2,128)(2,1)S(1)} %get-tuple-element.22, bf16[1,1024]{1,0:T(2,128)(2,1)S(1)} %get-tuple-element.23), kind=kOutput, calls=%fused_computation.8 | convolution fusion | flops 6311936 | bytes 2105344 | tf_op jit(solution)/shard_map/dot_general | solution.py:283
  105.0 2.4 %all-gather.1 = bf16[16,16,1024]{2,1,0:T(8,128)(2,1)S(1)} all-gather(bf16[8,16,1024]{2,1,0:T(8,128)(2,1)S(1)} %all-to-all-done.4), channel_id=3, replica_groups=mesh['y'=4,'xh'=2,'xl'=2,'z'=8,'c'=2] {'c'}, dimensions={0}, use_global_device_ids=true | all-gather | bytes 786432 | tf_op jit(solution)/shard_map/all_gather | solution.py:30
  108.9 3.1 %collective-permute-start.7 = (bf16[72,1024]{1,0:T(8,128)(2,1)S(1)}, bf16[72,1024]{1,0:T(8,128)(2,1)S(1)}, u32[]{:S(2)}, u32[]{:S(2)}) collective-permute-start(bf16[72,1024]{1,0:T(8,128)(2,1)S(1)} %get-tuple-element.15), channel_id=1, source_target_pairs={{0,128},{64,192},{128,0},{192,64},{1,129},{65,193},{129,1},{193,65... | collective-permute-start | bytes 442376 | tf_op jit(solution)/shard_map/ppermute | solution.py:299
  112.5 2.7 %collective-permute-start.9 = (bf16[72,1024]{1,0:T(8,128)(2,1)S(1)}, bf16[72,1024]{1,0:T(8,128)(2,1)S(1)}, u32[]{:S(2)}, u32[]{:S(2)}) collective-permute-start(bf16[72,1024]{1,0:T(8,128)(2,1)S(1)} %get-tuple-element.16), channel_id=1, source_target_pairs={{0,192},{64,0},{128,64},{192,128},{1,193},{65,1},{129,65},{193,129... | collective-permute-start | bytes 442376 | tf_op jit(solution)/shard_map/ppermute | solution.py:299
  115.2 3.0 %collective-permute-start.14 = (bf16[1024,256]{1,0:T(8,128)(2,1)}, bf16[1024,256]{1,0:T(8,128)(2,1)S(1)}, u32[]{:S(2)}, u32[]{:S(2)}) collective-permute-start(bf16[1024,256]{1,0:T(8,128)(2,1)} %collective-permute-done.13.after), channel_id=1, source_target_pairs={{0,48},{16,0},{32,16},{48,32},{1,49},{17,1},{33,17},{49,33},{2,50}... | collective-permute-start | bytes 1572872 | tf_op jit(solution)/shard_map/ppermute | solution.py:115
  120.1 2.2 %collective-permute-start.10 = (bf16[72,1024]{1,0:T(8,128)(2,1)S(1)}, bf16[72,1024]{1,0:T(8,128)(2,1)S(1)}, u32[]{:S(2)}, u32[]{:S(2)}) collective-permute-start(bf16[72,1024]{1,0:T(8,128)(2,1)S(1)} %fusion.20), channel_id=1, source_target_pairs={{0,128},{64,192},{128,0},{192,64},{1,129},{65,193},{129,1},{193,65... | collective-permute-start | bytes 442376 | tf_op jit(solution)/shard_map/ppermute | solution.py:313
  122.2 7.5 %collective-permute-done.15.before = bf16[1024,256]{1,0:T(8,128)(2,1)S(1)} collective-permute-done((bf16[1024,256]{1,0:T(8,128)(2,1)}, bf16[1024,256]{1,0:T(8,128)(2,1)S(1)}, u32[]{:S(2)}, u32[]{:S(2)}) %collective-permute-start.15) | collective-permute-done | bytes 524320 | tf_op jit(solution)/shard_map/ppermute | solution.py:113
  131.3 2.9 %shard_map.157 = bf16[1024,1024]{1,0:T(8,128)(2,1)} custom-call(bf16[1024,256]{1,0:T(8,128)(2,1)} %own.3, bf16[1024,256]{1,0:T(8,128)(2,1)} %collective-permute-done.13.after, bf16[1024,256]{1,0:T(8,128)(2,1)} %copy-done.8, bf16[1024,256]{1,0:T(8,128)(2,1)} %copy-done.7), custom_call_target="tpu_custom_call" | custom-call | tf_op jit(solution)/shard_map/pallas_call | solution.py:73
  134.3 3.2 %collective-permute-start.12 = (bf16[72,1024]{1,0:T(8,128)(2,1)S(1)}, bf16[72,1024]{1,0:T(8,128)(2,1)S(1)}, u32[]{:S(2)}, u32[]{:S(2)}) collective-permute-start(bf16[72,1024]{1,0:T(8,128)(2,1)S(1)} %fusion.20), channel_id=1, source_target_pairs={{0,192},{64,0},{128,64},{192,128},{1,193},{65,1},{129,65},{193,129... | collective-permute-start | bytes 442376 | tf_op jit(solution)/shard_map/ppermute | solution.py:313
  137.7 3.0 %collective-permute-done.11 = bf16[72,1024]{1,0:T(8,128)(2,1)S(1)} collective-permute-done((bf16[72,1024]{1,0:T(8,128)(2,1)S(1)}, bf16[72,1024]{1,0:T(8,128)(2,1)S(1)}, u32[]{:S(2)}, u32[]{:S(2)}) %collective-permute-start.11) | collective-permute-done | bytes 147488 | tf_op jit(solution)/shard_map/ppermute | solution.py:313
  141.6 1.5 collective-permute-done.16
  143.9 3.4 %all-to-all-start.5 = ((bf16[8,16,1024]{2,1,0:T(8,128)(2,1)}), bf16[8,16,1024]{2,1,0:T(8,128)(2,1)S(1)}, u32[]{:S(2)}, u32[]{:S(2)}) async-start(bf16[8,16,1024]{2,1,0:T(8,128)(2,1)} %bitcast.39), calls=%async_computation.5 | async-start | bytes 524288 | tf_op jit(solution)/shard_map/all_to_all | solution.py:42
  147.6 12.1 %all-to-all-done.5 = bf16[8,16,1024]{2,1,0:T(8,128)(2,1)S(1)} async-done(((bf16[8,16,1024]{2,1,0:T(8,128)(2,1)}), bf16[8,16,1024]{2,1,0:T(8,128)(2,1)S(1)}, u32[]{:S(2)}, u32[]{:S(2)}) %all-to-all-start.5) | async-done | bytes 262176 | tf_op jit(solution)/shard_map/all_to_all | solution.py:42
  160.2 15.9 %all_to_all.35 = bf16[16,16,384]{2,1,0:T(8,128)(2,1)S(1)} all-to-all(bf16[16,16,384]{2,1,0:T(8,128)(2,1)S(1)} %bitcast.142), channel_id=1, replica_groups=mesh['y'=4,'xh'=2,'xl'=2,'z'=8,'c'=2] {'xl','y','xh'}, dimensions={0} | all-to-all | bytes 393216 | tf_op jit(solution)/shard_map/all_to_all | solution.py:329
  (150 shorter events, 23.2 us)
Async XLA Ops:
  1.5 20.3 %all-to-all-start = ((bf16[8,64,256]{2,1,0:T(8,128)(2,1)}), bf16[8,64,256]{2,1,0:T(8,128)(2,1)S(1)}, u32[]{:S(2)}, u32[]{:S(2)}) async-start(bf16[8,64,256]{2,1,0:T(8,128)(2,1)} %broadcast_in_dim.90), calls=%async_computation | async-start | bytes 524288 | tf_op jit(solution)/shard_map/all_to_all | solution.py:25
  24.0 9.1 %copy-start.13 = (s32[64]{0:T(128)S(1)}, s32[64]{0:T(128)}, u32[]{:S(2)}) copy-start(s32[64]{0:T(128)} %param.17) | copy-start | bytes 772
  24.0 24.5 %copy-start = (bf16[64,128,128]{2,1,0:T(8,128)(2,1)S(1)}, bf16[64,128,128]{2,1,0:T(8,128)(2,1)}, u32[]{:S(2)}) copy-start(bf16[64,128,128]{2,1,0:T(8,128)(2,1)} %keys.1) | copy-start | bytes 6291460
  24.0 24.5 %copy-start.1 = (bf16[64,256]{1,0:T(8,128)(2,1)S(1)}, bf16[64,256]{1,0:T(8,128)(2,1)}, u32[]{:S(2)}) copy-start(bf16[64,256]{1,0:T(8,128)(2,1)} %tokens.1) | copy-start | bytes 98308
  25.4 23.1 %all-to-all-start.1 = ((bf16[16,64,512]{2,1,0:T(8,128)(2,1)}), bf16[16,64,512]{2,1,0:T(8,128)(2,1)S(1)}, u32[]{:S(2)}, u32[]{:S(2)}) async-start(bf16[16,64,512]{2,1,0:T(8,128)(2,1)} %bitcast.137), calls=%async_computation.1 | async-start | bytes 2097152 | tf_op jit(solution)/shard_map/all_to_all | solution.py:242
  33.5 25.4 %copy-start.12 = (f32[256]{0:T(256)S(1)}, f32[256]{0:T(256)}, u32[]{:S(2)}) copy-start(f32[256]{0:T(256)} %param.28) | copy-start | bytes 3076
  33.5 25.5 %copy-start.10 = (bf16[128,256]{1,0:T(8,128)(2,1)S(1)}, bf16[128,256]{1,0:T(8,128)(2,1)}, u32[]{:S(2)}) copy-start(bf16[128,256]{1,0:T(8,128)(2,1)} %param.27) | copy-start | bytes 196612
  52.9 15.8 %copy-start.4 = (bf16[256,1024]{1,0:T(8,128)(2,1)S(1)}, bf16[256,1024]{1,0:T(8,128)(2,1)}, u32[]{:S(2)}) copy-start(bf16[256,1024]{1,0:T(8,128)(2,1)} %own.2) | copy-start | bytes 1572868
  52.9 15.4 %all-to-all-start.2 = ((bf16[16,16,384]{2,1,0:T(8,128)(2,1)}), bf16[16,16,384]{2,1,0:T(8,128)(2,1)S(1)}, u32[]{:S(2)}, u32[]{:S(2)}) async-start(bf16[16,16,384]{2,1,0:T(8,128)(2,1)} %bitcast.4), calls=%async_computation.2 | async-start | bytes 393216 | tf_op jit(solution)/shard_map/all_to_all | solution.py:270
  59.1 4.4 %collective-permute-start.1 = (bf16[136,256]{1,0:T(8,128)(2,1)S(1)}, bf16[136,256]{1,0:T(8,128)(2,1)S(1)}, u32[]{:S(2)}, u32[]{:S(2)}) collective-permute-start(bf16[136,256]{1,0:T(8,128)(2,1)S(1)} %concatenate.85.own), channel_id=1, source_target_pairs={{0,16},{16,32},{32,48},{48,0},{1,17},{17,33},{33,49},{49,1},{2,18}... | collective-permute-start | bytes 208904 | tf_op jit(solution)/shard_map/ppermute | solution.py:113
  60.6 4.5 %collective-permute-start = (bf16[136,256]{1,0:T(8,128)(2,1)S(1)}, bf16[136,256]{1,0:T(8,128)(2,1)S(1)}, u32[]{:S(2)}, u32[]{:S(2)}) collective-permute-start(bf16[136,256]{1,0:T(8,128)(2,1)S(1)} %concatenate.85.own), channel_id=1, source_target_pairs={{0,48},{16,0},{32,16},{48,32},{1,49},{17,1},{33,17},{49,33},{2,50}... | collective-permute-start | bytes 208904 | tf_op jit(solution)/shard_map/ppermute | solution.py:114
  63.4 4.8 %collective-permute-start.2 = (bf16[136,256]{1,0:T(8,128)(2,1)S(1)}, bf16[136,256]{1,0:T(8,128)(2,1)S(1)}, u32[]{:S(2)}, u32[]{:S(2)}) collective-permute-start(bf16[136,256]{1,0:T(8,128)(2,1)S(1)} %collective-permute-done.1.before), channel_id=1, source_target_pairs={{0,16},{16,32},{32,48},{48,0},{1,17},{17,33},{33,49},{49,1},{2,18}... | collective-permute-start | bytes 208904 | tf_op jit(solution)/shard_map/ppermute | solution.py:115
  68.6 1.6 collective-permute-start.3
  68.7 15.8 %collective-permute-start.5 = (bf16[256,1024]{1,0:T(8,128)(2,1)S(1)}, bf16[256,1024]{1,0:T(8,128)(2,1)S(1)}, u32[]{:S(2)}, u32[]{:S(2)}) collective-permute-start(bf16[256,1024]{1,0:T(8,128)(2,1)S(1)} %copy-done.4), channel_id=1, source_target_pairs={{0,16},{16,32},{32,48},{48,0},{1,17},{17,33},{33,49},{49,1},{2,18}... | collective-permute-start | bytes 1572872 | tf_op jit(solution)/shard_map/ppermute | solution.py:113
  71.0 15.8 %all-to-all-start.3 = ((bf16[8,16,1024]{2,1,0:T(8,128)(2,1)}), bf16[8,16,1024]{2,1,0:T(8,128)(2,1)S(1)}, u32[]{:S(2)}, u32[]{:S(2)}) async-start(bf16[8,16,1024]{2,1,0:T(8,128)(2,1)} %bitcast.14), calls=%async_computation.3 | async-start | bytes 524288 | tf_op jit(solution)/shard_map/all_to_all | solution.py:42
  74.4 21.2 %collective-permute-start.4 = (bf16[256,1024]{1,0:T(8,128)(2,1)S(1)}, bf16[256,1024]{1,0:T(8,128)(2,1)S(1)}, u32[]{:S(2)}, u32[]{:S(2)}) collective-permute-start(bf16[256,1024]{1,0:T(8,128)(2,1)S(1)} %copy-done.4), channel_id=1, source_target_pairs={{0,48},{16,0},{32,16},{48,32},{1,49},{17,1},{33,17},{49,33},{2,50}... | collective-permute-start | bytes 1572872 | tf_op jit(solution)/shard_map/ppermute | solution.py:114
  84.5 14.6 %copy-start.5 = (bf16[256,1024]{1,0:T(8,128)(2,1)}, bf16[256,1024]{1,0:T(8,128)(2,1)S(1)}, u32[]{:S(2)}) copy-start(bf16[256,1024]{1,0:T(8,128)(2,1)S(1)} %collective-permute-done.5.before) | copy-start | bytes 1572868
  84.5 14.6 %collective-permute-start.6 = (bf16[256,1024]{1,0:T(8,128)(2,1)S(1)}, bf16[256,1024]{1,0:T(8,128)(2,1)S(1)}, u32[]{:S(2)}, u32[]{:S(2)}) collective-permute-start(bf16[256,1024]{1,0:T(8,128)(2,1)S(1)} %collective-permute-done.5.before), channel_id=1, source_target_pairs={{0,16},{16,32},{32,48},{48,0},{1,17},{17,33},{33,49},{49,1},{2,18}... | collective-permute-start | bytes 1572872 | tf_op jit(solution)/shard_map/ppermute | solution.py:115
  87.6 17.4 %all-to-all-start.4 = ((bf16[8,16,1024]{2,1,0:T(8,128)(2,1)}), bf16[8,16,1024]{2,1,0:T(8,128)(2,1)S(1)}, u32[]{:S(2)}, u32[]{:S(2)}) async-start(bf16[8,16,1024]{2,1,0:T(8,128)(2,1)} %broadcast_in_dim.98), calls=%async_computation.4 | async-start | bytes 524288 | tf_op jit(solution)/shard_map/all_to_all | solution.py:25
  91.0 24.2 %collective-permute-start.13 = (bf16[1024,256]{1,0:T(8,128)(2,1)}, bf16[1024,256]{1,0:T(8,128)(2,1)}, u32[]{:S(2)}, u32[]{:S(2)}) collective-permute-start(bf16[1024,256]{1,0:T(8,128)(2,1)} %own.3), channel_id=1, source_target_pairs={{0,48},{16,0},{32,16},{48,32},{1,49},{17,1},{33,17},{49,33},{2,50}... | collective-permute-start | bytes 1572872 | tf_op jit(solution)/shard_map/ppermute | solution.py:114
  108.9 9.3 %collective-permute-start.7 = (bf16[72,1024]{1,0:T(8,128)(2,1)S(1)}, bf16[72,1024]{1,0:T(8,128)(2,1)S(1)}, u32[]{:S(2)}, u32[]{:S(2)}) collective-permute-start(bf16[72,1024]{1,0:T(8,128)(2,1)S(1)} %get-tuple-element.15), channel_id=1, source_target_pairs={{0,128},{64,192},{128,0},{192,64},{1,129},{65,193},{129,1},{193,65... | collective-permute-start | bytes 442376 | tf_op jit(solution)/shard_map/ppermute | solution.py:299
  112.0 7.6 %collective-permute-start.8 = (bf16[72,1024]{1,0:T(8,128)(2,1)S(1)}, bf16[72,1024]{1,0:T(8,128)(2,1)S(1)}, u32[]{:S(2)}, u32[]{:S(2)}) collective-permute-start(bf16[72,1024]{1,0:T(8,128)(2,1)S(1)} %get-tuple-element.17), channel_id=1, source_target_pairs={{0,64},{64,128},{128,192},{192,0},{1,65},{65,129},{129,193},{193,1... | collective-permute-start | bytes 442376 | tf_op jit(solution)/shard_map/ppermute | solution.py:299
  112.5 7.1 %collective-permute-start.9 = (bf16[72,1024]{1,0:T(8,128)(2,1)S(1)}, bf16[72,1024]{1,0:T(8,128)(2,1)S(1)}, u32[]{:S(2)}, u32[]{:S(2)}) collective-permute-start(bf16[72,1024]{1,0:T(8,128)(2,1)S(1)} %get-tuple-element.16), channel_id=1, source_target_pairs={{0,192},{64,0},{128,64},{192,128},{1,193},{65,1},{129,65},{193,129... | collective-permute-start | bytes 442376 | tf_op jit(solution)/shard_map/ppermute | solution.py:299
  115.2 14.5 %collective-permute-start.15 = (bf16[1024,256]{1,0:T(8,128)(2,1)}, bf16[1024,256]{1,0:T(8,128)(2,1)S(1)}, u32[]{:S(2)}, u32[]{:S(2)}) collective-permute-start(bf16[1024,256]{1,0:T(8,128)(2,1)} %own.3), channel_id=1, source_target_pairs={{0,16},{16,32},{32,48},{48,0},{1,17},{17,33},{33,49},{49,1},{2,18}... | collective-permute-start | bytes 1572872 | tf_op jit(solution)/shard_map/ppermute | solution.py:113
  115.2 14.5 %collective-permute-start.14 = (bf16[1024,256]{1,0:T(8,128)(2,1)}, bf16[1024,256]{1,0:T(8,128)(2,1)S(1)}, u32[]{:S(2)}, u32[]{:S(2)}) collective-permute-start(bf16[1024,256]{1,0:T(8,128)(2,1)} %collective-permute-done.13.after), channel_id=1, source_target_pairs={{0,48},{16,0},{32,16},{48,32},{1,49},{17,1},{33,17},{49,33},{2,50}... | collective-permute-start | bytes 1572872 | tf_op jit(solution)/shard_map/ppermute | solution.py:115
  120.1 17.5 %collective-permute-start.10 = (bf16[72,1024]{1,0:T(8,128)(2,1)S(1)}, bf16[72,1024]{1,0:T(8,128)(2,1)S(1)}, u32[]{:S(2)}, u32[]{:S(2)}) collective-permute-start(bf16[72,1024]{1,0:T(8,128)(2,1)S(1)} %fusion.20), channel_id=1, source_target_pairs={{0,128},{64,192},{128,0},{192,64},{1,129},{65,193},{129,1},{193,65... | collective-permute-start | bytes 442376 | tf_op jit(solution)/shard_map/ppermute | solution.py:313
  134.2 6.5 %copy-start.2 = (bf16[1024,1024]{1,0:T(8,128)(2,1)S(1)}, bf16[1024,1024]{1,0:T(8,128)(2,1)}, u32[]{:S(2)}) copy-start(bf16[1024,1024]{1,0:T(8,128)(2,1)} %shard_map.157) | copy-start | bytes 6291460
  134.2 6.4 %collective-permute-start.11 = (bf16[72,1024]{1,0:T(8,128)(2,1)S(1)}, bf16[72,1024]{1,0:T(8,128)(2,1)S(1)}, u32[]{:S(2)}, u32[]{:S(2)}) collective-permute-start(bf16[72,1024]{1,0:T(8,128)(2,1)S(1)} %fusion.20), channel_id=1, source_target_pairs={{0,64},{64,128},{128,192},{192,0},{1,65},{65,129},{129,193},{193,1... | collective-permute-start | bytes 442376 | tf_op jit(solution)/shard_map/ppermute | solution.py:313
  134.3 6.4 %collective-permute-start.12 = (bf16[72,1024]{1,0:T(8,128)(2,1)S(1)}, bf16[72,1024]{1,0:T(8,128)(2,1)S(1)}, u32[]{:S(2)}, u32[]{:S(2)}) collective-permute-start(bf16[72,1024]{1,0:T(8,128)(2,1)S(1)} %fusion.20), channel_id=1, source_target_pairs={{0,192},{64,0},{128,64},{192,128},{1,193},{65,1},{129,65},{193,129... | collective-permute-start | bytes 442376 | tf_op jit(solution)/shard_map/ppermute | solution.py:313
  141.5 35.0 %copy-start.11 = (f32[256]{0:T(256)S(1)}, f32[256]{0:T(256)}, u32[]{:S(2)}) copy-start(f32[256]{0:T(256)} %param.31) | copy-start | bytes 3076
  141.5 1.6 collective-permute-start.16
  143.9 15.8 %all-to-all-start.5 = ((bf16[8,16,1024]{2,1,0:T(8,128)(2,1)}), bf16[8,16,1024]{2,1,0:T(8,128)(2,1)S(1)}, u32[]{:S(2)}, u32[]{:S(2)}) async-start(bf16[8,16,1024]{2,1,0:T(8,128)(2,1)} %bitcast.39), calls=%async_computation.5 | async-start | bytes 524288 | tf_op jit(solution)/shard_map/all_to_all | solution.py:42
  (5 other events, 10.9 us)

commit v3 on v2

--- a/solution.py
+++ b/solution.py
@@ -122,7 +122,7 @@
 
 
 def retain_kernel(
-    came, angles, heads, matrices, tokens, keys, values_from, state_from, sent, values, state, sems
+    came, angles, heads, matrices, keys, values_from, state_from, sent, values, state, sems
 ):
     groups = []
     for i in range(4):
@@ -176,13 +176,11 @@
     normed = centred * lax.rsqrt(variance + EPS) * gain
     mixed = (jax.nn.silu(gated.astype(F32)) * normed).astype(BF16)
     for x in range(4):
-        rows = pl.ds(16 * x, 16)
         for y in range(4):
-            sent[x % 2, y, x // 2, :, :128] = mixed[16 * x : 16 * x + 16]
-            sent[x % 2, y, x // 2, :, 128:] = tokens[rows]
-
-
-def retain(came, lengths, state, keys, values, rate, gain, tokens):
+            sent[x % 2, y, x // 2] = mixed[16 * x : 16 * x + 16]
+
+
+def retain(came, lengths, state, keys, values, rate, gain):
     lane = jnp.arange(384)
     inverse = 10000.0 ** (-(lane % 32).astype(F32) / 32)
     angle = lengths.astype(F32)[:, None] * inverse[None]
@@ -197,12 +195,11 @@
         angles,
         jnp.stack([jnp.repeat(rate, HDIM), gain]),
         jnp.concatenate([swap, ones]),
-        tokens,
     )
     sent = pl.pallas_call(
         retain_kernel,
-        out_shape=jax.ShapeDtypeStruct((2, 4, 2, 16, 384), BF16),
-        in_specs=[pl.BlockSpec(memory_space=pltpu.VMEM)] * 6
+        out_shape=jax.ShapeDtypeStruct((2, 4, 2, 16, 128), BF16),
+        in_specs=[pl.BlockSpec(memory_space=pltpu.VMEM)] * 5
         + [pl.BlockSpec(memory_space=pl.ANY)] * 2,
         out_specs=pl.BlockSpec(memory_space=pltpu.VMEM),
         scratch_shapes=[
@@ -212,7 +209,7 @@
         ],
         compiler_params=pltpu.CompilerParams(vmem_limit_bytes=52000000),
     )(*arrays, keys, values, state)
-    return sent.reshape(16, 16, 384)
+    return sent.reshape(16, 16, 128)
 
 
 def per_device(
@@ -248,7 +245,6 @@
         cached_values,
         decay_rate,
         head_gain,
-        tokens,
     )
     packed = jnp.concatenate(
         [out_weight, jnp.stack(apart(mixer_gain) + (jnp.zeros((256,), BF16),) * 5)]
@@ -268,8 +264,14 @@
     place = lax.axis_index(X)
 
     came = lax.all_to_all(sent, KV_ROWS, 0, 0, tiled=True)
-    mixed_rows = came[:, :, :128].reshape(256, 128)
-    token_rows = rolled(own_y(came[:, :, 128:]), place).swapaxes(0, 1).reshape(16, 1024)
+    mixed_rows = came.reshape(256, 128)
+    quarters = tokens.reshape(4, 16, 256)
+    token_slots = [lax.dynamic_index_in_dim(quarters, place, 0, keepdims=False)]
+    for d in (3, 2, 1):
+        piece = lax.dynamic_index_in_dim(quarters, (place + d) % 4, 0, keepdims=False)
+        came = lax.ppermute(piece, X, [(i, (i + d) % 4) for i in range(4)])
+        token_slots.append(came)
+    token_rows = jnp.concatenate(token_slots, 1)
 
     partial = jnp.dot(mixed_rows, out_rel, preferred_element_type=F32)
     branch = scatter_tp(partial)
@@ -303,19 +305,22 @@
     inverse = lax.rsqrt(sums[1] / 4096 - mean * mean + EPS)
     upward = (total[:64] - mean[:, None] * total[64:65]) * inverse[:, None]
     active = jnp.square(jax.nn.relu(upward)).astype(BF16)
-    stat_parts = jnp.stack(apart(jnp.stack([mean, inverse]))).reshape(1, 384)
-    block = jnp.concatenate(
-        [active, jnp.pad(stat_parts, ((0, 7), (0, 640)))]
-    )
-    came = jnp.zeros((4, 72, 1024), BF16)
-    came = lax.dynamic_update_index_in_dim(came, block, here, 0)
+    everyone = jnp.zeros((4, 64, 1024), BF16)
+    everyone = lax.dynamic_update_index_in_dim(everyone, active, here, 0)
     for d in (2, 1, 3):
-        piece = lax.ppermute(block, "y", [(i, (i + d) % 4) for i in range(4)])
-        came = lax.dynamic_update_index_in_dim(came, piece, (here - d) % 4, 0)
-    downward = scatter_tp(
-        jnp.dot(came[:, :64].reshape(256, 1024), down_rel, preferred_element_type=F32)
-    )
-    stats = came[:, 64, :384].astype(F32).reshape(4, 3, 2, 64).sum(1)
+        piece = lax.ppermute(active, "y", [(i, (i + d) % 4) for i in range(4)])
+        everyone = lax.dynamic_update_index_in_dim(everyone, piece, (here - d) % 4, 0)
+    partial = jnp.dot(everyone.reshape(256, 1024), down_rel, preferred_element_type=F32)
+    downward = scatter_tp(partial)
+    own_stats = jnp.pad(
+        jnp.stack(apart(jnp.stack([mean, inverse]))).reshape(3, 128), ((0, 5), (0, 0))
+    )
+    stats = jnp.zeros((4, 8, 128), BF16)
+    stats = lax.dynamic_update_index_in_dim(stats, own_stats, here, 0)
+    for d in (2, 1, 3):
+        piece = lax.ppermute(own_stats, "y", [(i, (i + d) % 4) for i in range(4)])
+        stats = lax.dynamic_update_index_in_dim(stats, piece, (here - d) % 4, 0)
+    stats = stats[:, :3].astype(F32).sum(1).reshape(4, 2, 64)
     stats = stats.swapaxes(0, 1).reshape(2, 16, 16)
     index = lax.axis_index("c") * 8 + lax.axis_index("z")
     mean, inverse = lax.dynamic_index_in_dim(stats, index, 1, keepdims=False)

time: 179 us -> 178 us (level)
  waiting for transfers between devices: 68.4 us -> 56.1 us
  starting transfers between devices: 58.4 us -> 66.4 us
  other arithmetic: 6.43 us -> 8.91 us
    ppermute x3, waiting for transfers between devices: 16.6 us -> 2.99 us  [x_slots(): before = lax.ppermute(x, X, forward)]
    ppermute x3 -> x9, starting transfers between devices: 5.46 us -> 13.2 us  [the longest x3 5.68 us: per_device(): piece = lax.ppermute(own_stats, 'y', [(i, (i + d) % 4) for i in range(4)])]
    ppermute x2, waiting for transfers between devices: 6.58 us -> 0.01 us  [x_slots(): lax.ppermute(before, X, forward)]
    all_to_all x1, waiting for transfers between devices: 0.01 us -> 5.54 us  [per_device(): came = lax.all_to_all(sent, KV_ROWS, 0, 0, tiled=True)]
    ppermute x3 -> x9, waiting for transfers between devices: 2.99 us -> 7.22 us  [the longest x3 4.19 us: per_device(): came = lax.ppermute(piece, X, [(i, (i + d) % 4) for i in range(4)])]
    ppermute x3, starting transfers between devices: 7.19 us -> 3.16 us  [x_slots(): after = lax.ppermute(x, X, back)]
    all_to_all x2, starting transfers between devices: 6.82 us -> 10.6 us  [scatter_tp(): parts = lax.all_to_all(pair.reshape(8, -1, n), 'z', 0, 0, tiled=True)]
    all_to_all x2, waiting for transfers between devices: 9.42 us -> 5.65 us  [copy_for_each(): lax.all_to_all(jnp.broadcast_to(x[None], (peers, *x.shape)), axis, 0, 0,...]
  transfers between devices with their start and end apart: 23 -> 29, of which waited for: 14 -> 13; matrix products, arithmetic and copies ran while one was open for 6% -> 10% of each run, Pallas kernels for 3% -> 6%
where the time goes in v3:
time: 178 us; the launch traced here: 177 us
  starting transfers between devices  66.4 us (37%)
  waiting for transfers between devices  56.1 us (32%)
  blocking collectives  19.5 us (11%)
  Pallas kernels  11 us (6%)
  other arithmetic  8.91 us (5%)
  local copies, waits for them, and re-layouts  8.84 us (5%)
  matrix products  5.83 us (3%)
    all_to_all x2, starting transfers between devices, copy_for_each(): lax.all_to_all(jnp.broadcast_to(x[None], (peers, *x.shape)), axis, 0, 0,...  15.5 us
    all_to_all x2, waiting for transfers between devices, scatter_tp(): parts = lax.all_to_all(pair.reshape(8, -1, n), 'z', 0, 0, tiled=True)  15.2 us
    all_to_all x1, blocking collectives, per_device(): lax.all_to_all(to_peers(jnp.concatenate([pieces, sums_sent], 2)), KV_ROWS...  15.2 us
    all_to_all x1, waiting for transfers between devices, per_device(): lax.all_to_all(partial.reshape(16, 64, 512), KV_ROWS, 0, 0, tiled=True)  13.4 us
    all_to_all x2, starting transfers between devices, scatter_tp(): parts = lax.all_to_all(pair.reshape(8, -1, n), 'z', 0, 0, tiled=True)  10.6 us
    all_to_all x1, starting transfers between devices, per_device(): lax.all_to_all(partial.reshape(16, 64, 512), KV_ROWS, 0, 0, tiled=True)  7.48 us
    all_to_all x1, starting transfers between devices, per_device(): came = lax.all_to_all(sent, KV_ROWS, 0, 0, tiled=True)  6.04 us
    pallas_call x2, Pallas kernels, copied(): pl.pallas_call(kernel, out_shape=out_shape, in_specs=[pl.BlockSpec(memory...  5.82 us
  transfers between devices with their start and end apart: 29, of which 13 were waited for; matrix products, arithmetic and copies ran while one was open for 10% of the time, Pallas kernels for 6%

profile of v3, /device:TPU:2, one launch (start us, length us, event | category | flops | bytes accessed | tf_op | source)
XLA Modules:
  0.0 177.3 jit_solution(2600226340766459694)
XLA Ops:
  0.0 1.5 broadcast_in_dim.106
  1.5 8.5 %all-to-all-start = ((bf16[8,64,256]{2,1,0:T(8,128)(2,1)}), bf16[8,64,256]{2,1,0:T(8,128)(2,1)S(1)}, u32[]{:S(2)}, u32[]{:S(2)}) async-start(bf16[8,64,256]{2,1,0:T(8,128)(2,1)} %broadcast_in_dim.106), calls=%async_computation | async-start | bytes 524288 | tf_op jit(solution)/shard_map/all_to_all | solution.py:25
  11.5 1.6 collective-permute-start.4
  16.2 5.6 %all-to-all-done = bf16[8,64,256]{2,1,0:T(8,128)(2,1)S(1)} async-done(((bf16[8,64,256]{2,1,0:T(8,128)(2,1)}), bf16[8,64,256]{2,1,0:T(8,128)(2,1)S(1)}, u32[]{:S(2)}, u32[]{:S(2)}) %all-to-all-start) | async-done | bytes 262176 | tf_op jit(solution)/shard_map/all_to_all | solution.py:25
  21.8 2.2 %all-gather = bf16[16,64,256]{2,1,0:T(8,128)(2,1)S(1)} all-gather(bf16[8,64,256]{2,1,0:T(8,128)(2,1)S(1)} %all-to-all-done), channel_id=2, replica_groups=mesh['y'=4,'xh'=2,'xl'=2,'z'=8,'c'=2] {'c'}, dimensions={0}, use_global_device_ids=true | all-gather | bytes 786432 | tf_op jit(solution)/shard_map/all_gather | solution.py:30
  25.4 7.5 %all-to-all-start.1 = ((bf16[16,64,512]{2,1,0:T(8,128)(2,1)}), bf16[16,64,512]{2,1,0:T(8,128)(2,1)S(1)}, u32[]{:S(2)}, u32[]{:S(2)}) async-start(bf16[16,64,512]{2,1,0:T(8,128)(2,1)} %bitcast.150), calls=%async_computation.1 | async-start | bytes 2097152 | tf_op jit(solution)/shard_map/all_to_all | solution.py:239
  33.5 1.5 collective-permute-start.5
  35.0 13.4 %all-to-all-done.1.came = bf16[16,64,512]{2,1,0:T(8,128)(2,1)S(1)} async-done(((bf16[16,64,512]{2,1,0:T(8,128)(2,1)}), bf16[16,64,512]{2,1,0:T(8,128)(2,1)S(1)}, u32[]{:S(2)}, u32[]{:S(2)}) %all-to-all-start.1) | async-done | bytes 1048608 | tf_op jit(solution)/shard_map/all_to_all | solution.py:239
  48.5 4.3 %shard_map.154 = bf16[2,4,2,16,128]{4,3,2,1,0:T(8,128)(2,1)} custom-call(bf16[16,64,512]{2,1,0:T(8,128)(2,1)S(1)} %all-to-all-done.1.came, f32[64,384]{1,0:T(8,128)S(1)} %fusion.19.angles, f32[2,128]{1,0:T(2,128)S(1)} %pad_maximum_fusion.4.heads, bf16[256,128]{1,0:T(8,128)(2,1)S(1)} %add_convert_fusion.matrices, bf16[64,128,128]{2,1,0:T(8,128)(2,1)S(1)} %copy-done, ...), custom_call_target="tpu_custom_call" | custom-call | tf_op jit(solution)/shard_map/pallas_call | solution.py:199
  52.8 6.0 %all-to-all-start.2 = ((bf16[16,16,128]{2,1,0:T(8,128)(2,1)}), bf16[16,16,128]{2,1,0:T(8,128)(2,1)S(1)}, u32[]{:S(2)}, u32[]{:S(2)}) async-start(bf16[16,16,128]{2,1,0:T(8,128)(2,1)} %bitcast.12), calls=%async_computation.2 | async-start | bytes 131072 | tf_op jit(solution)/shard_map/all_to_all | solution.py:266
  59.8 5.5 %all-to-all-done.2 = bf16[16,16,128]{2,1,0:T(8,128)(2,1)S(1)} async-done(((bf16[16,16,128]{2,1,0:T(8,128)(2,1)}), bf16[16,16,128]{2,1,0:T(8,128)(2,1)S(1)}, u32[]{:S(2)}, u32[]{:S(2)}) %all-to-all-start.2) | async-done | bytes 65568 | tf_op jit(solution)/shard_map/all_to_all | solution.py:266
  68.1 3.4 %all-to-all-start.3 = ((bf16[8,16,1024]{2,1,0:T(8,128)(2,1)}), bf16[8,16,1024]{2,1,0:T(8,128)(2,1)S(1)}, u32[]{:S(2)}, u32[]{:S(2)}) async-start(bf16[8,16,1024]{2,1,0:T(8,128)(2,1)} %bitcast.17), calls=%async_computation.3 | async-start | bytes 524288 | tf_op jit(solution)/shard_map/all_to_all | solution.py:42
  71.6 1.5 collective-permute-start
  73.1 1.8 %collective-permute-start.7 = (bf16[256,1024]{1,0:T(8,128)(2,1)S(1)}, bf16[256,1024]{1,0:T(8,128)(2,1)S(1)}, u32[]{:S(2)}, u32[]{:S(2)}) collective-permute-start(bf16[256,1024]{1,0:T(8,128)(2,1)S(1)} %copy-done.3), channel_id=1, source_target_pairs={{0,48},{16,0},{32,16},{48,32},{1,49},{17,1},{33,17},{49,33},{2,50}... | collective-permute-start | bytes 1572872 | tf_op jit(solution)/shard_map/ppermute | solution.py:114
  77.3 3.0 %collective-permute-done.8.before = bf16[256,1024]{1,0:T(8,128)(2,1)S(1)} collective-permute-done((bf16[256,1024]{1,0:T(8,128)(2,1)S(1)}, bf16[256,1024]{1,0:T(8,128)(2,1)S(1)}, u32[]{:S(2)}, u32[]{:S(2)}) %collective-permute-start.8) | collective-permute-done | bytes 524320 | tf_op jit(solution)/shard_map/ppermute | solution.py:113
  80.6 3.3 %all-to-all-done.3 = bf16[8,16,1024]{2,1,0:T(8,128)(2,1)S(1)} async-done(((bf16[8,16,1024]{2,1,0:T(8,128)(2,1)}), bf16[8,16,1024]{2,1,0:T(8,128)(2,1)S(1)}, u32[]{:S(2)}, u32[]{:S(2)}) %all-to-all-start.3) | async-done | bytes 262176 | tf_op jit(solution)/shard_map/all_to_all | solution.py:42
  83.9 4.2 %collective-permute-done.1 = bf16[16,256]{1,0:T(8,128)(2,1)S(1)} collective-permute-done((bf16[16,256]{1,0:T(8,128)(2,1)S(1)}, bf16[16,256]{1,0:T(8,128)(2,1)S(1)}, u32[]{:S(2)}, u32[]{:S(2)}) %collective-permute-start.1) | collective-permute-done | bytes 8224 | tf_op jit(solution)/shard_map/ppermute | solution.py:272
  88.9 7.1 %all-to-all-start.4 = ((bf16[8,16,1024]{2,1,0:T(8,128)(2,1)}), bf16[8,16,1024]{2,1,0:T(8,128)(2,1)S(1)}, u32[]{:S(2)}, u32[]{:S(2)}) async-start(bf16[8,16,1024]{2,1,0:T(8,128)(2,1)} %broadcast_in_dim.114), calls=%async_computation.4 | async-start | bytes 524288 | tf_op jit(solution)/shard_map/all_to_all | solution.py:25
  98.5 2.0 %collective-permute-start.20 = (bf16[1024,256]{1,0:T(8,128)(2,1)}, bf16[1024,256]{1,0:T(8,128)(2,1)}, u32[]{:S(2)}, u32[]{:S(2)}) collective-permute-start(bf16[1024,256]{1,0:T(8,128)(2,1)} %collective-permute-done.19.after), channel_id=1, source_target_pairs={{0,48},{16,0},{32,16},{48,32},{1,49},{17,1},{33,17},{49,33},{2,50}... | collective-permute-start | bytes 1572872 | tf_op jit(solution)/shard_map/ppermute | solution.py:115
  102.1 2.9 %shard_map.156 = bf16[1024,1024]{1,0:T(8,128)(2,1)} custom-call(bf16[256,1024]{1,0:T(8,128)(2,1)} %own.2, bf16[256,1024]{1,0:T(8,128)(2,1)} %copy-done.6, bf16[256,1024]{1,0:T(8,128)(2,1)} %copy-done.7, bf16[256,1024]{1,0:T(8,128)(2,1)} %copy-done.5), custom_call_target="tpu_custom_call" | custom-call | tf_op jit(solution)/shard_map/pallas_call | solution.py:73
  105.0 2.7 %convolution_reduce_fusion = bf16[1024]{0:T(1024)(128)(2,1)} fusion(bf16[1024,1024]{1,0:T(8,128)(2,1)} %shard_map.156, bf16[1,1024]{1,0:T(2,128)(2,1)S(1)} %get-tuple-element.26, bf16[1,1024]{1,0:T(2,128)(2,1)S(1)} %get-tuple-element.27, bf16[1,1024]{1,0:T(2,128)(2,1)S(1)} %get-tuple-element.28), kind=kOutput, calls=%fused_computation.8 | convolution fusion | flops 6311936 | bytes 2105344 | tf_op jit(solution)/shard_map/dot_general | solution.py:285
  107.7 2.2 %all-gather.1 = bf16[16,16,1024]{2,1,0:T(8,128)(2,1)S(1)} all-gather(bf16[8,16,1024]{2,1,0:T(8,128)(2,1)S(1)} %all-to-all-done.4), channel_id=3, replica_groups=mesh['y'=4,'xh'=2,'xl'=2,'z'=8,'c'=2] {'c'}, dimensions={0}, use_global_device_ids=true | all-gather | bytes 786432 | tf_op jit(solution)/shard_map/all_gather | solution.py:30
  114.2 2.4 %collective-permute-start.12 = (bf16[72,1024]{1,0:T(8,128)(2,1)S(1)}, bf16[72,1024]{1,0:T(8,128)(2,1)}, u32[]{:S(2)}, u32[]{:S(2)}) collective-permute-start(bf16[72,1024]{1,0:T(8,128)(2,1)S(1)} %get-tuple-element.16), channel_id=1, source_target_pairs={{0,192},{64,0},{128,64},{192,128},{1,193},{65,1},{129,65},{193,129... | collective-permute-start | bytes 442376 | tf_op jit(solution)/shard_map/ppermute | solution.py:301
  116.6 2.9 %shard_map.157 = bf16[1024,1024]{1,0:T(8,128)(2,1)} custom-call(bf16[1024,256]{1,0:T(8,128)(2,1)} %own.3, bf16[1024,256]{1,0:T(8,128)(2,1)} %collective-permute-done.19.after, bf16[1024,256]{1,0:T(8,128)(2,1)} %collective-permute-done.20.far, bf16[1024,256]{1,0:T(8,128)(2,1)} %collective-permute-done.21.before), custom_call_target="tpu_custom_call" | custom-call | tf_op jit(solution)/shard_map/pallas_call | solution.py:73
  120.8 2.3 %collective-permute-done.11 = bf16[72,1024]{1,0:T(8,128)(2,1)} collective-permute-done((bf16[72,1024]{1,0:T(8,128)(2,1)}, bf16[72,1024]{1,0:T(8,128)(2,1)}, u32[]{:S(2)}, u32[]{:S(2)}) %collective-permute-start.11) | collective-permute-done | bytes 147488 | tf_op jit(solution)/shard_map/ppermute | solution.py:301
  125.9 2.4 %collective-permute-start.13 = (bf16[8,128]{1,0:T(8,128)(2,1)S(1)}, bf16[8,128]{1,0:T(8,128)(2,1)S(1)}, u32[]{:S(2)}, u32[]{:S(2)}) collective-permute-start(bf16[8,128]{1,0:T(8,128)(2,1)S(1)} %fusion.46), channel_id=1, source_target_pairs={{0,128},{64,192},{128,0},{192,64},{1,129},{65,193},{129,1},{193,65... | collective-permute-start | bytes 6152 | tf_op jit(solution)/shard_map/ppermute | solution.py:321
  128.9 2.7 %collective-permute-start.15 = (bf16[8,128]{1,0:T(8,128)(2,1)S(1)}, bf16[8,128]{1,0:T(8,128)(2,1)S(1)}, u32[]{:S(2)}, u32[]{:S(2)}) collective-permute-start(bf16[8,128]{1,0:T(8,128)(2,1)S(1)} %fusion.46), channel_id=1, source_target_pairs={{0,192},{64,0},{128,64},{192,128},{1,193},{65,1},{129,65},{193,129... | collective-permute-start | bytes 6152 | tf_op jit(solution)/shard_map/ppermute | solution.py:321
  131.7 3.1 %collective-permute-start.18 = (bf16[64,1024]{1,0:T(8,128)(2,1)S(1)}, bf16[64,1024]{1,0:T(8,128)(2,1)S(1)}, u32[]{:S(2)}, u32[]{:S(2)}) collective-permute-start(bf16[64,1024]{1,0:T(8,128)(2,1)S(1)} %get-tuple-element.14), channel_id=1, source_target_pairs={{0,192},{64,0},{128,64},{192,128},{1,193},{65,1},{129,65},{193,129... | collective-permute-start | bytes 393224 | tf_op jit(solution)/shard_map/ppermute | solution.py:311
  134.9 2.9 %collective-permute-done.17 = bf16[64,1024]{1,0:T(8,128)(2,1)S(1)} collective-permute-done((bf16[64,1024]{1,0:T(8,128)(2,1)S(1)}, bf16[64,1024]{1,0:T(8,128)(2,1)S(1)}, u32[]{:S(2)}, u32[]{:S(2)}) %collective-permute-start.17) | collective-permute-done | bytes 131104 | tf_op jit(solution)/shard_map/ppermute | solution.py:311
  141.0 7.2 %all-to-all-start.5 = ((bf16[8,16,1024]{2,1,0:T(8,128)(2,1)}), bf16[8,16,1024]{2,1,0:T(8,128)(2,1)S(1)}, u32[]{:S(2)}, u32[]{:S(2)}) async-start(bf16[8,16,1024]{2,1,0:T(8,128)(2,1)} %bitcast.47), calls=%async_computation.5 | async-start | bytes 524288 | tf_op jit(solution)/shard_map/all_to_all | solution.py:42
  148.5 11.9 %all-to-all-done.5 = bf16[8,16,1024]{2,1,0:T(8,128)(2,1)S(1)} async-done(((bf16[8,16,1024]{2,1,0:T(8,128)(2,1)}), bf16[8,16,1024]{2,1,0:T(8,128)(2,1)S(1)}, u32[]{:S(2)}, u32[]{:S(2)}) %all-to-all-start.5) | async-done | bytes 262176 | tf_op jit(solution)/shard_map/all_to_all | solution.py:42
  161.0 15.2 %all_to_all.35 = bf16[16,16,384]{2,1,0:T(8,128)(2,1)S(1)} all-to-all(bf16[16,16,384]{2,1,0:T(8,128)(2,1)S(1)} %bitcast.155), channel_id=1, replica_groups=mesh['y'=4,'xh'=2,'xl'=2,'z'=8,'c'=2] {'xl','y','xh'}, dimensions={0} | all-to-all | bytes 393216 | tf_op jit(solution)/shard_map/all_to_all | solution.py:334
  (159 shorter events, 31.8 us)
Async XLA Ops:
  1.5 20.3 %all-to-all-start = ((bf16[8,64,256]{2,1,0:T(8,128)(2,1)}), bf16[8,64,256]{2,1,0:T(8,128)(2,1)S(1)}, u32[]{:S(2)}, u32[]{:S(2)}) async-start(bf16[8,64,256]{2,1,0:T(8,128)(2,1)} %broadcast_in_dim.106), calls=%async_computation | async-start | bytes 524288 | tf_op jit(solution)/shard_map/all_to_all | solution.py:25
  11.5 21.9 %collective-permute-start.4 = (bf16[136,256]{1,0:T(8,128)(2,1)S(1)}, bf16[136,256]{1,0:T(8,128)(2,1)S(1)}, u32[]{:S(2)}, u32[]{:S(2)}) collective-permute-start(bf16[136,256]{1,0:T(8,128)(2,1)S(1)} %concatenate.83.own), channel_id=1, source_target_pairs={{0,16},{16,32},{32,48},{48,0},{1,17},{17,33},{33,49},{49,1},{2,18}... | collective-permute-start | bytes 208904 | tf_op jit(solution)/shard_map/ppermute | solution.py:113
  13.1 45.8 %collective-permute-start.3 = (bf16[136,256]{1,0:T(8,128)(2,1)S(1)}, bf16[136,256]{1,0:T(8,128)(2,1)S(1)}, u32[]{:S(2)}, u32[]{:S(2)}) collective-permute-start(bf16[136,256]{1,0:T(8,128)(2,1)S(1)} %concatenate.83.own), channel_id=1, source_target_pairs={{0,48},{16,0},{32,16},{48,32},{1,49},{17,1},{33,17},{49,33},{2,50}... | collective-permute-start | bytes 208904 | tf_op jit(solution)/shard_map/ppermute | solution.py:114
  24.0 24.5 %copy-start = (bf16[64,128,128]{2,1,0:T(8,128)(2,1)S(1)}, bf16[64,128,128]{2,1,0:T(8,128)(2,1)}, u32[]{:S(2)}) copy-start(bf16[64,128,128]{2,1,0:T(8,128)(2,1)} %keys.1) | copy-start | bytes 6291460
  25.4 23.1 %all-to-all-start.1 = ((bf16[16,64,512]{2,1,0:T(8,128)(2,1)}), bf16[16,64,512]{2,1,0:T(8,128)(2,1)S(1)}, u32[]{:S(2)}, u32[]{:S(2)}) async-start(bf16[16,64,512]{2,1,0:T(8,128)(2,1)} %bitcast.150), calls=%async_computation.1 | async-start | bytes 2097152 | tf_op jit(solution)/shard_map/all_to_all | solution.py:239
  33.5 25.4 %collective-permute-start.5 = (bf16[136,256]{1,0:T(8,128)(2,1)S(1)}, bf16[136,256]{1,0:T(8,128)(2,1)}, u32[]{:S(2)}, u32[]{:S(2)}) collective-permute-start(bf16[136,256]{1,0:T(8,128)(2,1)S(1)} %collective-permute-done.4.before), channel_id=1, source_target_pairs={{0,16},{16,32},{32,48},{48,0},{1,17},{17,33},{33,49},{49,1},{2,18}... | collective-permute-start | bytes 208904 | tf_op jit(solution)/shard_map/ppermute | solution.py:115
  52.8 23.7 %copy-start.4 = (bf16[1024,256]{1,0:T(8,128)(2,1)S(1)}, bf16[1024,256]{1,0:T(8,128)(2,1)}, u32[]{:S(2)}) copy-start(bf16[1024,256]{1,0:T(8,128)(2,1)} %own.3) | copy-start | bytes 1572868
  52.8 12.5 %all-to-all-start.2 = ((bf16[16,16,128]{2,1,0:T(8,128)(2,1)}), bf16[16,16,128]{2,1,0:T(8,128)(2,1)S(1)}, u32[]{:S(2)}, u32[]{:S(2)}) async-start(bf16[16,16,128]{2,1,0:T(8,128)(2,1)} %bitcast.12), calls=%async_computation.2 | async-start | bytes 131072 | tf_op jit(solution)/shard_map/all_to_all | solution.py:266
  65.7 1.6 collective-permute-start.6
  65.8 14.5 %collective-permute-start.8 = (bf16[256,1024]{1,0:T(8,128)(2,1)S(1)}, bf16[256,1024]{1,0:T(8,128)(2,1)S(1)}, u32[]{:S(2)}, u32[]{:S(2)}) collective-permute-start(bf16[256,1024]{1,0:T(8,128)(2,1)S(1)} %copy-done.3), channel_id=1, source_target_pairs={{0,16},{16,32},{32,48},{48,0},{1,17},{17,33},{33,49},{49,1},{2,18}... | collective-permute-start | bytes 1572872 | tf_op jit(solution)/shard_map/ppermute | solution.py:113
  68.1 15.8 %all-to-all-start.3 = ((bf16[8,16,1024]{2,1,0:T(8,128)(2,1)}), bf16[8,16,1024]{2,1,0:T(8,128)(2,1)S(1)}, u32[]{:S(2)}, u32[]{:S(2)}) async-start(bf16[8,16,1024]{2,1,0:T(8,128)(2,1)} %bitcast.17), calls=%async_computation.3 | async-start | bytes 524288 | tf_op jit(solution)/shard_map/all_to_all | solution.py:42
  71.6 4.9 %collective-permute-start = (bf16[16,256]{1,0:T(8,128)(2,1)S(1)}, bf16[16,256]{1,0:T(8,128)(2,1)S(1)}, u32[]{:S(2)}, u32[]{:S(2)}) collective-permute-start(bf16[16,256]{1,0:T(8,128)(2,1)S(1)} %get-tuple-element.22), channel_id=1, source_target_pairs={{0,48},{16,0},{32,16},{48,32},{1,49},{17,1},{33,17},{49,33},{2,50}... | collective-permute-start | bytes 24584 | tf_op jit(solution)/shard_map/ppermute | solution.py:272
  73.1 27.4 %collective-permute-start.7 = (bf16[256,1024]{1,0:T(8,128)(2,1)S(1)}, bf16[256,1024]{1,0:T(8,128)(2,1)S(1)}, u32[]{:S(2)}, u32[]{:S(2)}) collective-permute-start(bf16[256,1024]{1,0:T(8,128)(2,1)S(1)} %copy-done.3), channel_id=1, source_target_pairs={{0,48},{16,0},{32,16},{48,32},{1,49},{17,1},{33,17},{49,33},{2,50}... | collective-permute-start | bytes 1572872 | tf_op jit(solution)/shard_map/ppermute | solution.py:114
  74.9 13.2 %collective-permute-start.1 = (bf16[16,256]{1,0:T(8,128)(2,1)S(1)}, bf16[16,256]{1,0:T(8,128)(2,1)S(1)}, u32[]{:S(2)}, u32[]{:S(2)}) collective-permute-start(bf16[16,256]{1,0:T(8,128)(2,1)S(1)} %get-tuple-element.21), channel_id=1, source_target_pairs={{0,32},{16,48},{32,0},{48,16},{1,33},{17,49},{33,1},{49,17},{2,34}... | collective-permute-start | bytes 24584 | tf_op jit(solution)/shard_map/ppermute | solution.py:272
  75.2 13.0 %collective-permute-start.2 = (bf16[16,256]{1,0:T(8,128)(2,1)S(1)}, bf16[16,256]{1,0:T(8,128)(2,1)S(1)}, u32[]{:S(2)}, u32[]{:S(2)}) collective-permute-start(bf16[16,256]{1,0:T(8,128)(2,1)S(1)} %get-tuple-element.20), channel_id=1, source_target_pairs={{0,16},{16,32},{32,48},{48,0},{1,17},{17,33},{33,49},{49,1},{2,18}... | collective-permute-start | bytes 24584 | tf_op jit(solution)/shard_map/ppermute | solution.py:272
  76.5 22.0 %collective-permute-start.19 = (bf16[1024,256]{1,0:T(8,128)(2,1)S(1)}, bf16[1024,256]{1,0:T(8,128)(2,1)}, u32[]{:S(2)}, u32[]{:S(2)}) collective-permute-start(bf16[1024,256]{1,0:T(8,128)(2,1)S(1)} %copy-done.4), channel_id=1, source_target_pairs={{0,48},{16,0},{32,16},{48,32},{1,49},{17,1},{33,17},{49,33},{2,50}... | collective-permute-start | bytes 1572872 | tf_op jit(solution)/shard_map/ppermute | solution.py:114
  80.3 20.2 %collective-permute-start.9 = (bf16[256,1024]{1,0:T(8,128)(2,1)S(1)}, bf16[256,1024]{1,0:T(8,128)(2,1)S(1)}, u32[]{:S(2)}, u32[]{:S(2)}) collective-permute-start(bf16[256,1024]{1,0:T(8,128)(2,1)S(1)} %collective-permute-done.8.before), channel_id=1, source_target_pairs={{0,16},{16,32},{32,48},{48,0},{1,17},{17,33},{33,49},{49,1},{2,18}... | collective-permute-start | bytes 1572872 | tf_op jit(solution)/shard_map/ppermute | solution.py:115
  88.9 18.9 %all-to-all-start.4 = ((bf16[8,16,1024]{2,1,0:T(8,128)(2,1)}), bf16[8,16,1024]{2,1,0:T(8,128)(2,1)S(1)}, u32[]{:S(2)}, u32[]{:S(2)}) async-start(bf16[8,16,1024]{2,1,0:T(8,128)(2,1)} %broadcast_in_dim.114), calls=%async_computation.4 | async-start | bytes 524288 | tf_op jit(solution)/shard_map/all_to_all | solution.py:25
  95.9 20.7 %collective-permute-start.21 = (bf16[1024,256]{1,0:T(8,128)(2,1)S(1)}, bf16[1024,256]{1,0:T(8,128)(2,1)}, u32[]{:S(2)}, u32[]{:S(2)}) collective-permute-start(bf16[1024,256]{1,0:T(8,128)(2,1)S(1)} %copy-done.4), channel_id=1, source_target_pairs={{0,16},{16,32},{32,48},{48,0},{1,17},{17,33},{33,49},{49,1},{2,18}... | collective-permute-start | bytes 1572872 | tf_op jit(solution)/shard_map/ppermute | solution.py:113
  98.5 18.1 %collective-permute-start.20 = (bf16[1024,256]{1,0:T(8,128)(2,1)}, bf16[1024,256]{1,0:T(8,128)(2,1)}, u32[]{:S(2)}, u32[]{:S(2)}) collective-permute-start(bf16[1024,256]{1,0:T(8,128)(2,1)} %collective-permute-done.19.after), channel_id=1, source_target_pairs={{0,48},{16,0},{32,16},{48,32},{1,49},{17,1},{33,17},{49,33},{2,50}... | collective-permute-start | bytes 1572872 | tf_op jit(solution)/shard_map/ppermute | solution.py:115
  112.2 8.6 %collective-permute-start.10 = (bf16[72,1024]{1,0:T(8,128)(2,1)}, bf16[72,1024]{1,0:T(8,128)(2,1)}, u32[]{:S(2)}, u32[]{:S(2)}) collective-permute-start(bf16[72,1024]{1,0:T(8,128)(2,1)} %get-tuple-element.15), channel_id=1, source_target_pairs={{0,128},{64,192},{128,0},{192,64},{1,129},{65,193},{129,1},{193,65... | collective-permute-start | bytes 442376 | tf_op jit(solution)/shard_map/ppermute | solution.py:301
  113.4 9.7 %collective-permute-start.11 = (bf16[72,1024]{1,0:T(8,128)(2,1)}, bf16[72,1024]{1,0:T(8,128)(2,1)}, u32[]{:S(2)}, u32[]{:S(2)}) collective-permute-start(bf16[72,1024]{1,0:T(8,128)(2,1)} %get-tuple-element.17), channel_id=1, source_target_pairs={{0,64},{64,128},{128,192},{192,0},{1,65},{65,129},{129,193},{193,1... | collective-permute-start | bytes 442376 | tf_op jit(solution)/shard_map/ppermute | solution.py:301
  114.2 8.8 %collective-permute-start.12 = (bf16[72,1024]{1,0:T(8,128)(2,1)S(1)}, bf16[72,1024]{1,0:T(8,128)(2,1)}, u32[]{:S(2)}, u32[]{:S(2)}) collective-permute-start(bf16[72,1024]{1,0:T(8,128)(2,1)S(1)} %get-tuple-element.16), channel_id=1, source_target_pairs={{0,192},{64,0},{128,64},{192,128},{1,193},{65,1},{129,65},{193,129... | collective-permute-start | bytes 442376 | tf_op jit(solution)/shard_map/ppermute | solution.py:301
  124.7 7.1 %collective-permute-start.16 = (bf16[64,1024]{1,0:T(8,128)(2,1)S(1)}, bf16[64,1024]{1,0:T(8,128)(2,1)S(1)}, u32[]{:S(2)}, u32[]{:S(2)}) collective-permute-start(bf16[64,1024]{1,0:T(8,128)(2,1)S(1)} %get-tuple-element.14), channel_id=1, source_target_pairs={{0,128},{64,192},{128,0},{192,64},{1,129},{65,193},{129,1},{193,65... | collective-permute-start | bytes 393224 | tf_op jit(solution)/shard_map/ppermute | solution.py:311
  125.9 12.8 %collective-permute-start.13 = (bf16[8,128]{1,0:T(8,128)(2,1)S(1)}, bf16[8,128]{1,0:T(8,128)(2,1)S(1)}, u32[]{:S(2)}, u32[]{:S(2)}) collective-permute-start(bf16[8,128]{1,0:T(8,128)(2,1)S(1)} %fusion.46), channel_id=1, source_target_pairs={{0,128},{64,192},{128,0},{192,64},{1,129},{65,193},{129,1},{193,65... | collective-permute-start | bytes 6152 | tf_op jit(solution)/shard_map/ppermute | solution.py:321
  128.4 19.9 %collective-permute-start.14 = (bf16[8,128]{1,0:T(8,128)(2,1)S(1)}, bf16[8,128]{1,0:T(8,128)(2,1)S(1)}, u32[]{:S(2)}, u32[]{:S(2)}) collective-permute-start(bf16[8,128]{1,0:T(8,128)(2,1)S(1)} %fusion.46), channel_id=1, source_target_pairs={{0,64},{64,128},{128,192},{192,0},{1,65},{65,129},{129,193},{193,1... | collective-permute-start | bytes 6152 | tf_op jit(solution)/shard_map/ppermute | solution.py:321
  128.9 19.4 %collective-permute-start.15 = (bf16[8,128]{1,0:T(8,128)(2,1)S(1)}, bf16[8,128]{1,0:T(8,128)(2,1)S(1)}, u32[]{:S(2)}, u32[]{:S(2)}) collective-permute-start(bf16[8,128]{1,0:T(8,128)(2,1)S(1)} %fusion.46), channel_id=1, source_target_pairs={{0,192},{64,0},{128,64},{192,128},{1,193},{65,1},{129,65},{193,129... | collective-permute-start | bytes 6152 | tf_op jit(solution)/shard_map/ppermute | solution.py:321
  131.6 6.2 %collective-permute-start.17 = (bf16[64,1024]{1,0:T(8,128)(2,1)S(1)}, bf16[64,1024]{1,0:T(8,128)(2,1)S(1)}, u32[]{:S(2)}, u32[]{:S(2)}) collective-permute-start(bf16[64,1024]{1,0:T(8,128)(2,1)S(1)} %get-tuple-element.14), channel_id=1, source_target_pairs={{0,64},{64,128},{128,192},{192,0},{1,65},{65,129},{129,193},{193,1... | collective-permute-start | bytes 393224 | tf_op jit(solution)/shard_map/ppermute | solution.py:311
  131.7 6.1 %collective-permute-start.18 = (bf16[64,1024]{1,0:T(8,128)(2,1)S(1)}, bf16[64,1024]{1,0:T(8,128)(2,1)S(1)}, u32[]{:S(2)}, u32[]{:S(2)}) collective-permute-start(bf16[64,1024]{1,0:T(8,128)(2,1)S(1)} %get-tuple-element.14), channel_id=1, source_target_pairs={{0,192},{64,0},{128,64},{192,128},{1,193},{65,1},{129,65},{193,129... | collective-permute-start | bytes 393224 | tf_op jit(solution)/shard_map/ppermute | solution.py:311
  138.6 38.0 %copy-start.11 = (f32[256]{0:T(256)S(1)}, f32[256]{0:T(256)}, u32[]{:S(2)}) copy-start(f32[256]{0:T(256)} %param.31) | copy-start | bytes 3076
  138.6 1.6 collective-permute-start.22
  141.0 19.4 %all-to-all-start.5 = ((bf16[8,16,1024]{2,1,0:T(8,128)(2,1)}), bf16[8,16,1024]{2,1,0:T(8,128)(2,1)S(1)}, u32[]{:S(2)}, u32[]{:S(2)}) async-start(bf16[8,16,1024]{2,1,0:T(8,128)(2,1)} %bitcast.47), calls=%async_computation.5 | async-start | bytes 524288 | tf_op jit(solution)/shard_map/all_to_all | solution.py:42
  (11 other events, 96.4 us)
